TPU v7x, 256 devices: a whole 4x4x8 slice. The times are simulated.
256 devices in a mesh: sp: 64 (over z, y, core), tp: 4 (over x).
Axes of the slice: x: 4, y: 4, z: 8, core: 2. Of those that a mesh axis runs over, the one named last changes fastest.
Arguments:
- moe_input: bfloat16 [8192, 2048], P('sp', 'tp'), may hold values from -6 to 6
- cotangent: bfloat16 [8192, 2048], P('sp', 'tp'), may hold values from -16 to 16
- expert_ids: int32 [8192, 2], P('sp'), may hold values from 0 to 63, as said below
- routing_weights: float32 [8192, 2], P('sp'), may hold values from 0.1 to 0.6
- gate_weight: bfloat16 [64, 2048, 1024], P('sp', None, 'tp'), may hold values from -0.125 to 0.125
- up_weight: bfloat16 [64, 2048, 1024], P('sp', None, 'tp'), may hold values from -0.125 to 0.125
- down_weight: bfloat16 [64, 1024, 2048], P('sp', 'tp'), may hold values from -0.1875 to 0.1875
- inner_x: bfloat16 [8192, 4096], P('sp', 'tp'), may hold values from -6 to 6
- inner_b: bfloat16 [8192, 256], P('sp', 'tp'), may hold values from -6 to 6
- inner_c: bfloat16 [8192, 256], P('sp', 'tp'), may hold values from -6 to 6
- gate_z: bfloat16 [8192, 4096], P('sp', 'tp'), may hold values from -6 to 6
- step_raw: float32 [8192, 64], P('sp', 'tp'), may hold values from -30 to 2
- decay_rate: float32 [64], P('tp'), may hold values from 1 to 16
- skip_weight: float32 [64], P('tp'), may hold values from 0.1 to 1.9
- norm_gain: float32 [4096], P('tp'), may hold values from 0.1 to 1.9
- w_out: bfloat16 [2048, 4096], P(None, 'tp'), may hold values from -0.09375 to 0.09375
Outputs:
- gate_weight_gradient: bfloat16 [64, 2048, 1024], P('sp', None, 'tp')
- up_weight_gradient: bfloat16 [64, 2048, 1024], P('sp', None, 'tp')
- down_weight_gradient: bfloat16 [64, 1024, 2048], P('sp', 'tp')
- grad_out: float32 [2048, 4096], P('sp', 'tp')
- grad_inner_x: bfloat16 [8192, 4096], P('sp', 'tp')
- grad_inner_b: float32 [8192, 256], P('sp', 'tp')
- grad_inner_c: float32 [8192, 256], P('sp', 'tp')
- grad_gate_z: bfloat16 [8192, 4096], P('sp', 'tp')
- grad_step_raw: float32 [8192, 64], P('sp', 'tp')
Inputs may be any that keep to these rules, and one draw needn't show every extreme that they name: `expert_ids`: the two entries of a row differ and lie in the same group of 16 consecutive experts. In each aligned block of 128 rows no expert is named more than 8 times; one group of experts, the same for all blocks, takes exactly half of every block's rows, and each of its experts is named exactly 8 times in every block.
All inputs are finite; a program needn't handle non-finite values.
Results may differ from a plain program's by a relative error of at most 0.015.
Values may be sent and summed in bfloat16 or wider, within the bound.
No kernel may reach another device: no remote copies, remote signals or barrier semaphores. Data moves between devices by JAX's collectives and lax.ppermute only.
A program may use at most 128 MiB of HBM per device.

v0:
```python
import jax
import jax.numpy as jnp
from jax import lax
from jax.sharding import Mesh
from jax.experimental import pallas as pl
from jax.experimental.pallas import tpu as pltpu
from jax.sharding import PartitionSpec as P

HEAD_DIM = 64
STATE = 64
LANES = 128
SLOTS = 8
EPS = 0.01
SP = ("z", "y", "c")
F32 = jnp.float32
BF16 = jnp.bfloat16
HIGH = lax.Precision.HIGHEST


def along(value, axis, step):
    count = lax.axis_size(axis)
    return lax.ppermute(value, axis, [(i, (i + step) % count) for i in range(count)])


def shifted(value, step):
    return along(value, "x", step)


def to_all(value, axes):
    return lax.all_to_all(value, axes, split_axis=0, concat_axis=0, tiled=True)


def around(value):
    return shifted(value, 1), shifted(value, -1), shifted(value, 2)


def rows_of(tiled):
    cols = tiled.shape[1] // SLOTS
    rows = tiled.reshape(-1, cols, SLOTS, LANES).transpose(0, 2, 1, 3)
    return rows.reshape(-1, cols * LANES)


SMALL, LARGE = 1 << 30, 1 << 32


def softplus(value):
    small = jnp.exp(-jnp.abs(value))
    grown = 1.0 + small
    log_part = jnp.where(
        grown == 1.0, small, jnp.log(grown) * (small / jnp.where(grown == 1.0, 1.0, grown - 1.0))
    )
    return jnp.maximum(value, 0.0) + log_part


def sigmoid(value):
    return 1.0 / (1.0 + jnp.exp(-value))


def mm(left, right):
    return jnp.dot(left.astype(BF16), right.astype(BF16), preferred_element_type=F32)


def mm_nt(left, right):
    return lax.dot_general(
        left.astype(BF16),
        right.astype(BF16),
        (((1,), (1,)), ((), ())),
        preferred_element_type=F32,
    )


def exact(left, right):
    return jnp.dot(left, right, preferred_element_type=F32, precision=HIGH)


def iota(shape, dim):
    return lax.broadcasted_iota(jnp.int32, shape, dim)


def head_lanes(heads, wide):
    return ((iota((heads, wide), 1) >> 6) == iota((heads, wide), 0)).astype(F32)


def head_rows(heads, wide):
    return ((iota((wide, heads), 0) >> 6) == iota((wide, heads), 1)).astype(F32)


def clocks(raw_t, rate):
    step = softplus(raw_t).T
    logs = -step * rate
    tok = logs.shape[0]
    upto = (iota((tok, tok), 0) >= iota((tok, tok), 1)).astype(F32)
    return step, exact(upto, logs)


def routing(ids_t, experts):
    numbers = iota((experts, ids_t.shape[1]), 0)
    first, second = ids_t[0:1, :] == numbers, ids_t[1:2, :] == numbers
    named = jnp.where(first, 1.0, jnp.where(second, 1.0, 0.0))
    tok = ids_t.shape[1]
    earlier = (iota((tok, tok), 0) < iota((tok, tok), 1)).astype(F32)
    before = mm(named, earlier)
    key = jnp.where(named > 0.0, before, -1.0)
    shape = (experts, SLOTS, tok)
    pick = jnp.broadcast_to(key[:, None, :], shape) == iota(shape, 1).astype(F32)
    return first, second, jnp.where(pick, 1.0, 0.0)


def put_tiles(out_ref, rows, experts):
    cols = rows.shape[1] // LANES
    tiled = rows.reshape(experts, SLOTS, rows.shape[1])
    for col in range(cols):
        out_ref[:, col * SLOTS : (col + 1) * SLOTS, :] = tiled[
            :, :, col * LANES : (col + 1) * LANES
        ].astype(BF16)


def put_pieces(out_ref, at, state):
    rows = state.shape[0] // 8
    for col in range(state.shape[1] // LANES):
        piece = state[:, col * LANES : (col + 1) * LANES].reshape(rows, 8, LANES)
        out_ref[col * rows : (col + 1) * rows, at : at + 8, :] = piece.astype(BF16)


def get_pieces(pieces):
    rows = STATE // 8
    cols = pieces.shape[0] // rows
    return jnp.concatenate(
        [pieces[col * rows : (col + 1) * rows].reshape(STATE, LANES) for col in range(cols)],
        axis=1,
    )


def enter_kernel(ids_ref, moe_ref, out_ref):
    experts = out_ref.shape[0]
    pick = routing(ids_ref[...], experts)[2]
    put_tiles(out_ref, mm(pick.reshape(experts * SLOTS, -1), moe_ref[...]), experts)


def put_fresh(x_ref, b_ref, raw_ref, rate_ref, out_ref):
    step, running = clocks(raw_ref[...], rate_ref[...])
    heads, wide = step.shape[1], x_ref.shape[1]
    last = running[-1:, :]
    spread = exact(
        jnp.concatenate(
            [step * jnp.exp(last - running), jnp.broadcast_to(jnp.exp(last), (8, heads))], axis=0
        ),
        head_lanes(heads, wide),
    )
    x = x_ref[...].astype(F32)
    at_end = x * sigmoid(x) * spread[:-8]
    b = b_ref[...].astype(F32)
    put_pieces(out_ref, 32, mm(b * sigmoid(b), at_end))
    total = spread[-8:]
    high = total.astype(BF16).astype(F32)
    mid = (total - high).astype(BF16).astype(F32)
    low = total - high - mid
    row = iota(total.shape, 0)
    tile = jnp.where(row == 0, high, jnp.where(row == 1, mid, jnp.where(row == 2, low, 0.0)))
    rows_at = STATE // 8
    for col in range(wide // LANES):
        part = tile[:, col * LANES : (col + 1) * LANES].astype(BF16)
        out_ref[col * rows_at : (col + 1) * rows_at, 40:48, :] = jnp.broadcast_to(
            part[None], (rows_at, 8, LANES)
        )


def weigh_kernel(ids_ref, weights_ref, cot_ref, x_ref, b_ref, raw_ref, rate_ref, out_ref):
    put_fresh(x_ref, b_ref, raw_ref, rate_ref, out_ref)
    experts = out_ref.shape[0]
    first, second, pick = routing(ids_ref[...], experts)
    weights = weights_ref[...]
    weight_at = jnp.where(first, weights[0:1, :], 0.0) + jnp.where(second, weights[1:2, :], 0.0)
    scaling = jnp.sum(
        pick * jnp.broadcast_to(weight_at[:, None, :], pick.shape), axis=2, keepdims=True
    )
    rows = mm(pick.reshape(experts * SLOTS, -1), cot_ref[...])
    put_tiles(
        out_ref,
        (rows.reshape(experts, SLOTS, -1) * scaling).reshape(experts * SLOTS, -1),
        experts,
    )


def block_decays(got_ref):
    tile = got_ref[:, 40:48, :].astype(F32)
    total = tile[:, 0:1, :] + tile[:, 1:2, :] + tile[:, 2:3, :]
    return jnp.broadcast_to(total, tile.shape)


def ahead_kernel(got_ref, out_ref):
    decays = block_decays(got_ref)
    pieces = got_ref[:, 32:40, :].astype(F32)
    total = jnp.zeros(pieces.shape[1:], F32)
    found = []
    for k in range(pieces.shape[0]):
        found.append(total)
        total = total * decays[k] + pieces[k]
    out_ref[...] = jnp.stack(found, axis=0).astype(BF16)


def behind_kernel(got_ref, pieces_ref, out_ref):
    decays = block_decays(got_ref)
    pieces = pieces_ref[...].astype(F32)
    total = jnp.zeros(pieces.shape[1:], F32)
    found = []
    for k in reversed(range(pieces.shape[0])):
        found.append(total)
        total = total * decays[k] + pieces[k]
    out_ref[...] = jnp.stack(found[::-1], axis=0).astype(BF16)


def first_kernel(here_ref, own_ref, left_ref, right_ref, far_ref, gate_ref, up_ref, out_gate_ref, out_up_ref):
    here = here_ref[0]
    for weight_ref, out_ref in ((gate_ref, out_gate_ref), (up_ref, out_up_ref)):
        total = None
        for block_ref, offset in ((own_ref, 0), (left_ref, 3), (right_ref, 1), (far_ref, 2)):
            width = block_ref.shape[1]
            at = pl.multiple_of(((here + offset) & 3) * width, width)
            term = mm(block_ref[...], weight_ref[pl.ds(at, width), :])
            total = term if total is None else total + term
        out_ref[...] = total


def middle_kernel(
    here_ref, own_ref, left_ref, right_ref, op_ref, down_ref, pre_ref, up_pre_ref, gate_ref, up_ref,
    hidden_ref, gate_grad_ref, up_grad_ref, far_ref, next_ref, back_ref, rest_ref,
):
    here = here_ref[0]
    hidden_grad = None
    for block_ref, offset in ((own_ref, 0), (left_ref, 3), (right_ref, 1), (op_ref, 2)):
        width = block_ref.shape[1]
        at = pl.multiple_of(((here + offset) & 3) * width, width)
        term = mm_nt(block_ref[...], down_ref[:, pl.ds(at, width)])
        hidden_grad = term if hidden_grad is None else hidden_grad + term
    pre, up_pre = pre_ref[...], up_pre_ref[...]
    sig = sigmoid(pre)
    active = pre * sig
    hidden_ref[...] = (active * up_pre).astype(BF16)
    gate_grad = (hidden_grad * up_pre * sig * (1.0 + pre * (1.0 - sig))).astype(BF16)
    up_grad = (hidden_grad * active).astype(BF16)
    gate_grad_ref[...] = gate_grad
    up_grad_ref[...] = up_grad
    width = rest_ref.shape[1]
    for offset, term_ref in ((2, far_ref), (1, next_ref), (3, back_ref), (0, rest_ref)):
        at = pl.multiple_of(((here + offset) & 3) * width, width)
        term = mm_nt(gate_grad, gate_ref[pl.ds(at, width), :]) + mm_nt(
            up_grad, up_ref[pl.ds(at, width), :]
        )
        term_ref[...] = term.astype(BF16)


def weights_kernel(
    here_ref, in0_ref, in1_ref, in2_ref, in3_ref, out0_ref, out1_ref, out2_ref, out3_ref,
    hidden_ref, gate_grad_ref, up_grad_ref, gate_ref, up_ref, down_ref,
):
    here = here_ref[0]
    hidden_t = hidden_ref[...].T
    for in_ref, grad_ref, offset in (
        (in0_ref, out0_ref, 0), (in1_ref, out1_ref, 3), (in2_ref, out2_ref, 1), (in3_ref, out3_ref, 2)
    ):
        width = in_ref.shape[1]
        at = pl.multiple_of(((here + offset) & 3) * width, width)
        block_t = in_ref[...].T
        gate_ref[pl.ds(at, width), :] = mm(block_t, gate_grad_ref[...]).astype(BF16)
        up_ref[pl.ds(at, width), :] = mm(block_t, up_grad_ref[...]).astype(BF16)
        down_ref[:, pl.ds(at, width)] = mm(hidden_t, grad_ref[...]).astype(BF16)


def combine_kernel(ids_ref, cot_ref, back_ref, out_ref):
    experts = back_ref.shape[0] // SLOTS
    pick = routing(ids_ref[...], experts)[2].reshape(experts * SLOTS, -1)
    moe_grad = mm(pick.T, back_ref[...])
    rows = (cot_ref[...].astype(F32) + moe_grad).astype(BF16)
    for k in range(out_ref.shape[0]):
        out_ref[k] = rows


def halves(value):
    low = iota(value.shape, 1) < HEAD_DIM
    return jnp.where(low, value, 0.0), jnp.where(low, 0.0, value)


def fade_of(column, row, keep):
    return jnp.exp(jnp.where(keep, column - row, -1e30))


def forward_kernel(
    x_ref, z_ref, b_ref, c_ref, raw_ref, rate_ref, skip_ref, gain_ref, got_ref,
    norm_ref, mixed_ref, start_ref, wide_ref,
):
    start = get_pieces(got_ref[...].astype(F32))
    start_ref[...] = start.astype(BF16)
    step, running = clocks(raw_ref[...], rate_ref[...])
    tok, heads = step.shape
    wide = x_ref.shape[1]
    spread = exact(
        jnp.concatenate(
            [step, jnp.exp(running), jnp.broadcast_to(skip_ref[...], (8, heads))], axis=0
        ),
        head_lanes(heads, wide),
    )
    x = x_ref[...].astype(F32)
    x_act = x * sigmoid(x)
    scaled = x_act * spread[:tok]
    wide_ref[...] = spread[tok : 2 * tok]
    b, c = b_ref[...].astype(F32), c_ref[...].astype(F32)
    b_t, c_t = b * sigmoid(b), c * sigmoid(c)
    c_act = c_t.T
    scores = mm(c_act, b_t)
    mixed = spread[tok : 2 * tok] * mm(c_act, start) + x_act * spread[2 * tok : 2 * tok + 1]
    running_t = running.T
    keep = iota((tok, tok), 0) >= iota((tok, tok), 1)
    for pair in range(heads // 2):
        lanes = slice(pair * LANES, (pair + 1) * LANES)
        mixes = [
            scores * fade_of(running[:, h : h + 1], running_t[h : h + 1, :], keep)
            for h in (2 * pair, 2 * pair + 1)
        ]
        inside = mm(
            jnp.concatenate(mixes, axis=1), jnp.concatenate(halves(scaled[:, lanes]), axis=0)
        )
        mixed_ref[:, lanes] = mixed[:, lanes] + inside
    z = z_ref[...].astype(F32)
    gated = mixed_ref[...] * (z * sigmoid(z))
    scale = lax.rsqrt(jnp.mean(gated * gated, axis=1, keepdims=True) + EPS)
    norm_ref[...] = (gated * scale * gain_ref[...]).astype(BF16)


def gate_back_kernel(
    rows_ref, w_ref, mixed_ref, z_ref, gain_ref, wide_ref, c_ref, pieces_ref, grad_z_ref, d_mixed_ref
):
    z = z_ref[...].astype(F32)
    sig = sigmoid(z)
    z_act = z * sig
    mixed = mixed_ref[...]
    gated = mixed * z_act
    scale = lax.rsqrt(jnp.mean(gated * gated, axis=1, keepdims=True) + EPS)
    rows = jnp.concatenate([rows_ref[k] for k in range(rows_ref.shape[0])], axis=1)
    d_norm = mm(rows, w_ref[...]) * gain_ref[...]
    along_row = jnp.mean(d_norm * gated, axis=1, keepdims=True)
    d_gated = scale * d_norm - gated * (scale * scale * scale * along_row)
    d_mixed = d_gated * z_act
    c = c_ref[...].astype(F32)
    put_pieces(pieces_ref, 0, mm(c * sigmoid(c), d_mixed * wide_ref[...]))
    d_mixed_ref[...] = d_mixed
    grad_z_ref[...] = (d_gated * mixed * (sig * (1.0 + z * (1.0 - sig)))).astype(BF16)


def project_kernel(*refs):
    plane, row = refs[0][0], refs[0][1]
    part_refs, near_ref, far_ref = refs[1:5], refs[5], refs[6]
    own_ref, share_refs, left_ref = refs[7], refs[8:15], refs[15]
    tok = near_ref.shape[1]
    planes, rows = part_refs[0].shape[1], part_refs[0].shape[2]
    for step in range(planes):
        for k, part_ref in enumerate(part_refs):
            for half in (0, 1):
                at = (2 * k + half) * tok
                left_ref[step * rows : (step + 1) * rows, at : at + tok] = part_ref[
                    half, (plane + step) & (planes - 1)
                ]
    total = None
    for k in range(4):
        for half, block_ref in enumerate((near_ref, far_ref)):
            at = (2 * k + half) * tok
            term = mm(left_ref[:, at : at + tok], block_ref[(row - k) & 3])
            total = term if total is None else total + term
    own_ref[...] = total[:rows]
    for step in range(1, planes):
        share_refs[step - 1][...] = total[step * rows : (step + 1) * rows].astype(BF16)


def inside_back_kernel(
    x_ref, b_ref, c_ref, raw_ref, rate_ref, skip_ref, start_ref, wide_ref, d_mixed_ref,
    grad_x_ref, reach_x_ref, reach_s_ref, at_end_ref, d_b_ref, grad_c_ref, small_ref,
    d_scaled_ref,
):
    step, running = clocks(raw_ref[...], rate_ref[...])
    tok, heads = step.shape
    wide = x_ref.shape[1]
    last = running[-1:, :]
    spread = exact(
        jnp.concatenate(
            [step, jnp.exp(last - running), jnp.broadcast_to(skip_ref[...], (8, heads))], axis=0
        ),
        head_lanes(heads, wide),
    )
    step_wide, end_wide = spread[:tok], spread[tok : 2 * tok]
    x = x_ref[...].astype(F32)
    sig = sigmoid(x)
    x_act = x * sig
    scaled = x_act * step_wide
    d_mixed = d_mixed_ref[...]
    b, c = b_ref[...].astype(F32), c_ref[...].astype(F32)
    sig_c = sigmoid(c)
    b_t, c_t = b * sigmoid(b), c * sig_c
    b_act, c_act = b_t.T, c_t.T
    scores, scores_t = mm(c_act, b_t), mm(b_act, c_t)
    running_t = running.T
    rows, cols = iota((tok, tok), 0), iota((tok, tok), 1)
    keep, keep_t = rows >= cols, rows <= cols
    d_scores = jnp.zeros((tok, tok), F32)
    gained = jnp.zeros((tok, heads), F32)
    lost = jnp.zeros((heads, tok), F32)
    head_at, head_row = iota((tok, heads), 1), iota((heads, tok), 0)
    for pair in range(heads // 2):
        lanes = slice(pair * LANES, (pair + 1) * LANES)
        d_parts = halves(d_mixed[:, lanes])
        mixes_t = []
        for half in (0, 1):
            h = 2 * pair + half
            column, row = running[:, h : h + 1], running_t[h : h + 1, :]
            fade = fade_of(column, row, keep)
            mixes_t.append(scores_t * jnp.exp(jnp.where(keep_t, row - column, -1e30)))
            d_fade = mm_nt(d_parts[half], scaled[:, lanes]) * fade
            d_scores = d_scores + d_fade
            flow = d_fade * scores
            gained = jnp.where(head_at == h, jnp.sum(flow, axis=1, keepdims=True), gained)
            lost = jnp.where(head_row == h, jnp.sum(flow, axis=0, keepdims=True), lost)
        d_scaled_ref[:, lanes] = mm(
            jnp.concatenate(mixes_t, axis=1), jnp.concatenate(d_parts, axis=0)
        )
    start = start_ref[...].astype(F32)
    d_carried = d_mixed * wide_ref[...]
    by_head = head_rows(heads, wide)
    d_scaled = d_scaled_ref[...]
    d_run = gained - lost.T + exact(d_carried * mm(c_act, start), by_head)
    d_step = exact(d_scaled * x_act, by_head)
    small_ref[0] = d_run
    small_ref[1] = d_step
    small_ref[2] = jnp.broadcast_to(jnp.exp(last), (tok, heads))
    d_silu = sig * (1.0 + x * (1.0 - sig))
    grad_x_ref[...] = (d_scaled * step_wide + d_mixed * spread[2 * tok : 2 * tok + 1]) * d_silu
    reach_x_ref[...] = end_wide * step_wide * d_silu
    reach_s_ref[...] = end_wide * x_act
    at_end_ref[...] = (scaled * end_wide).astype(BF16)
    d_b_ref[...] = mm(c_t, d_scores)
    d_c = mm_nt(b_t, d_scores) + mm_nt(start, d_carried)
    grad_c_ref[...] = d_c * (sig_c * (1.0 + c * (1.0 - sig_c)))


def leave_kernel(
    pieces_ref, start_ref, b_ref, raw_ref, rate_ref, base_ref, reach_x_ref, reach_s_ref,
    at_end_ref, d_b_ref, small_ref, grad_x_ref, grad_b_ref, grad_step_ref,
):
    after = get_pieces(pieces_ref[...].astype(F32))
    b = b_ref[...].astype(F32)
    sig_b = sigmoid(b)
    reach = mm((b * sig_b).T, after)
    grad_x_ref[...] = (base_ref[...] + reach * reach_x_ref[...]).astype(BF16)
    tok, wide = reach.shape
    raw = raw_ref[...]
    step = softplus(raw).T
    heads = step.shape[1]
    both = jnp.concatenate(
        [
            reach * reach_s_ref[...],
            jnp.broadcast_to(
                jnp.sum(after * start_ref[...].astype(F32), axis=0, keepdims=True), (8, wide)
            ),
        ],
        axis=0,
    )
    sums = exact(both, head_rows(heads, wide))
    lost = step * sums[:tok]
    d_run = small_ref[0] - lost
    end_part = jnp.sum(lost, axis=0, keepdims=True) + small_ref[2][:1] * sums[tok : tok + 1]
    onward = (iota((tok, tok), 0) <= iota((tok, tok), 1)).astype(F32)
    d_log = exact(onward, d_run) + end_part
    d_step = small_ref[1] + sums[:tok] - d_log * rate_ref[...]
    grad_step_ref[...] = d_step.T * sigmoid(raw)
    d_b = d_b_ref[...] + mm_nt(after, at_end_ref[...])
    grad_b_ref[...] = d_b * (sig_b * (1.0 + b * (1.0 - sig_b)))


class Held:
    def __init__(self, array):
        self.array = array


def local(kernel, outs, args, flops, scratch=(), scalars=0, away=()):
    outs = outs if isinstance(outs, tuple) else (outs,)
    outs = tuple(pltpu.HBM(o.shape, o.dtype) if i in away else o for i, o in enumerate(outs))
    held = [i for i, a in enumerate(args) if isinstance(a, Held)]
    arrays = [
        pltpu.with_memory_space_constraint(a.array, pltpu.HBM) if isinstance(a, Held) else a
        for a in args
    ]
    spaces = [
        pltpu.SMEM if i < scalars else pltpu.HBM if i in held else pltpu.VMEM
        for i in range(len(args))
    ]
    count = len(args) + len(outs) + len(scratch)

    def run(*refs):
        refs, inside, sems = list(refs[:count]), refs[count:-1], refs[-1]
        copies = []
        for k, i in enumerate(held):
            copies.append(pltpu.make_async_copy(refs[i], inside[k], sems.at[k]))
            copies[-1].start()
            refs[i] = inside[k]
        for copy in copies:
            copy.wait()
        kernel(*refs)

    call = pl.pallas_call(
        run if held else kernel,
        out_shape=outs,
        scratch_shapes=(
            *scratch,
            *[pltpu.VMEM(arrays[i].shape, arrays[i].dtype) for i in held],
            *([pltpu.SemaphoreType.DMA((len(held),))] if held else []),
        ),
        in_specs=[pl.BlockSpec(memory_space=space) for space in spaces],
        compiler_params=pltpu.CompilerParams(vmem_limit_bytes=16 << 20),
        cost_estimate=pl.CostEstimate(flops=flops, bytes_accessed=1 << 21, transcendentals=1 << 18),
    )
    found = call(*arrays)
    return found if len(outs) > 1 else found[0]


def body(
    moe_input,
    cotangent,
    expert_ids,
    routing_weights,
    gate_weight,
    up_weight,
    down_weight,
    inner_x,
    inner_b,
    inner_c,
    gate_z,
    step_raw,
    decay_rate,
    skip_weight,
    norm_gain,
    w_out,
):
    tok = expert_ids.shape[0]
    heads = decay_rate.shape[0]
    experts = lax.axis_size(SP)
    wide = inner_x.shape[1]
    gate_w, up_w, down_w = gate_weight[0], up_weight[0], down_weight[0]
    ids_t, b_t, c_t, raw_t = expert_ids.T, inner_b.T, inner_c.T, step_raw.T
    rate, skip, gain = decay_rate[None, :], skip_weight[None, :], norm_gain[None, :]
    here = lax.axis_index("x")[None]
    shape = jax.ShapeDtypeStruct
    slots = experts * SLOTS
    cols, inner = moe_input.shape[1], gate_w.shape[1]

    sent_in = local(
        enter_kernel, shape((experts, 32, LANES), BF16), (Held(ids_t), Held(moe_input)), SMALL
    )
    got_in = to_all(sent_in, SP)
    sent_grad = local(
        weigh_kernel,
        shape((experts, 48, LANES), BF16),
        (Held(ids_t), Held(routing_weights.T), Held(cotangent), Held(inner_x), Held(b_t), Held(raw_t), Held(rate)),
        SMALL,
    )
    got_grad = to_all(sent_grad, SP)

    rows_in = rows_of(got_in)
    in_left, in_right, in_far = around(rows_in)
    pre, up_pre = local(
        first_kernel,
        (shape((slots, inner), F32), shape((slots, inner), F32)),
        (here, rows_in, in_left, in_right, in_far, Held(gate_w), Held(up_w)),
        SMALL,
        scalars=1,
        away=(0, 1),
    )
    rows_grad = rows_of(got_grad[:, :32])
    grad_left, grad_right, grad_far = around(rows_grad)

    pieces = local(ahead_kernel, shape((experts, 8, LANES), BF16), (got_grad,), SMALL)
    pieces = to_all(pieces, SP)

    hidden, gate_grad, up_grad, term_far, term_next, term_back, term_own = local(
        middle_kernel,
        (
            shape((slots, inner), BF16),
            shape((slots, inner), BF16),
            shape((slots, inner), BF16),
            *[shape((slots, cols), BF16)] * 4,
        ),
        (here, rows_grad, grad_left, grad_right, grad_far, Held(down_w), Held(pre), Held(up_pre), Held(gate_w), Held(up_w)),
        SMALL,
        scalars=1,
        away=(0, 1, 2),
    )
    terms = shifted(term_far, 2), shifted(term_next, 1), shifted(term_back, -1)
    slot_grad = term_own.astype(F32)
    for term in terms:
        slot_grad = slot_grad + term.astype(F32)
    slot_grad = slot_grad.astype(BF16)

    norm_rows, mixed, start_state, start_wide = local(
        forward_kernel,
        (
            shape((tok, wide), BF16),
            shape((tok, wide), F32),
            shape((STATE, wide), BF16),
            shape((tok, wide), F32),
        ),
        (Held(inner_x), Held(gate_z), Held(b_t), Held(c_t), Held(raw_t), Held(rate), Held(skip), Held(gain), pieces),
        SMALL,
        away=(1, 2, 3),
    )
    norm_y = to_all(jnp.broadcast_to(norm_rows[None], (4, tok, wide)), "y")
    slot_grad, norm_y = lax.optimization_barrier((slot_grad, norm_y))
    back = to_all(slot_grad.reshape(experts, SLOTS, -1), SP).reshape(slots, -1)
    norm_c = along(norm_y, "c", 1)
    gate_out, up_out, down_out = local(
        weights_kernel,
        (
            shape(gate_w.shape, BF16),
            shape(up_w.shape, BF16),
            shape(down_w.shape, BF16),
        ),
        (
            here,
            *[
                Held(a)
                for a in (
                    rows_in, in_left, in_right, in_far, rows_grad, grad_left, grad_right, grad_far,
                    hidden, gate_grad, up_grad,
                )
            ],
        ),
        LARGE,
        scalars=1,
    )

    mixer_cols = local(
        combine_kernel,
        shape((4, *cotangent.shape), BF16),
        (Held(ids_t), Held(cotangent), back),
        SMALL,
    )
    mixer4 = to_all(mixer_cols, "x")

    pieces, grad_z, d_mixed = local(
        gate_back_kernel,
        (
            shape((experts, 8, LANES), BF16),
            shape((tok, wide), BF16),
            shape((tok, wide), F32),
        ),
        (mixer4, Held(w_out), Held(mixed), Held(gate_z), Held(gain), Held(start_wide), Held(c_t)),
        SMALL,
        away=(2,),
    )

    mine, row, plane = lax.axis_index("c"), lax.axis_index("y"), lax.axis_index("z")
    mixer_t = mixer4.transpose(0, 2, 1).reshape(8, 4, 2, 32, tok).transpose(2, 1, 0, 3, 4)
    pieces = to_all(pieces, SP)
    keep = lax.dynamic_index_in_dim(mixer_t, mine, 0, keepdims=False)
    give = lax.dynamic_index_in_dim(mixer_t, 1 - mine, 0, keepdims=False)
    take = along(give, "c", 1)
    both = jnp.stack([keep, take], axis=0)
    parts = [lax.dynamic_index_in_dim(both, row, 1, keepdims=False)] + [
        along(lax.dynamic_index_in_dim(both, (row + step) % 4, 1, keepdims=False), "y", step)
        for step in (1, 2, 3)
    ]
    found = local(
        project_kernel,
        (shape((32, wide), F32), *[shape((32, wide), BF16)] * 7),
        (jnp.stack([plane, row]), *parts, norm_y, norm_c),
        SMALL,
        (pltpu.VMEM((256, 8 * tok), BF16),),
        scalars=1,
    )
    grad_out = found[0]
    for step in (4, 3, 5, 2, 6, 1, 7):
        share = along(found[step], "z", step)
        grad_out = grad_out + share.astype(F32)
    pieces = local(behind_kernel, shape((experts, 8, LANES), BF16), (got_grad, pieces), SMALL)
    pieces = to_all(pieces, SP)
    grad_x, reach_x, reach_s, at_end, d_b, grad_c, small = local(
        inside_back_kernel,
        (
            shape((tok, wide), F32),
            shape((tok, wide), F32),
            shape((tok, wide), F32),
            shape((tok, wide), BF16),
            shape((STATE, tok), F32),
            shape((STATE, tok), F32),
            shape((3, tok, heads), F32),
        ),
        (Held(inner_x), Held(b_t), Held(c_t), Held(raw_t), Held(rate), Held(skip), Held(start_state), Held(start_wide), Held(d_mixed)),
        LARGE,
        (pltpu.VMEM((tok, wide), F32),),
        away=tuple(range(7)),
    )
    grad_x, grad_b, grad_step = local(
        leave_kernel,
        (shape((tok, wide), BF16), shape((STATE, tok), F32), shape((heads, tok), F32)),
        (
            pieces,
            *[
                Held(a)
                for a in (start_state, b_t, raw_t, rate, grad_x, reach_x, reach_s, at_end, d_b, small)
            ],
        ),
        SMALL,
    )
    return (
        gate_out[None],
        up_out[None],
        down_out[None],
        grad_out,
        grad_x,
        grad_b.T,
        grad_c.T,
        grad_z,
        grad_step.T,
    )


def solution(mesh):
    finer = Mesh(mesh.devices.reshape(8, 4, 2, mesh.shape["tp"]), ("z", "y", "c", "x"))
    return jax.shard_map(
        body,
        mesh=finer,
        in_specs=(
            P(SP, "x"),
            P(SP, "x"),
            P(SP, None),
            P(SP, None),
            P(SP, None, "x"),
            P(SP, None, "x"),
            P(SP, "x", None),
            P(SP, "x"),
            P(SP, "x"),
            P(SP, "x"),
            P(SP, "x"),
            P(SP, "x"),
            P("x"),
            P("x"),
            P("x"),
            P(None, "x"),
        ),
        out_specs=(
            P(SP, None, "x"),
            P(SP, None, "x"),
            P(SP, "x", None),
            P(SP, "x"),
            P(SP, "x"),
            P(SP, "x"),
            P(SP, "x"),
            P(SP, "x"),
            P(SP, "x"),
        ),
        check_vma=False,
    )
```

profile of v0, /device:TPU:1, one launch (start us, length us, event | category | flops | bytes accessed | tf_op | source)
XLA Modules:
  0.0 230.3 jit_solution(414297652301484229)
XLA Ops:
  2.8 13.2 %all-to-all-start = ((bf16[64,32,128]{2,1,0:T(8,128)(2,1)}), bf16[64,32,128]{2,1,0:T(8,128)(2,1)S(1)}, u32[]{:S(2)}, u32[]{:S(2)}) async-start(bf16[64,32,128]{2,1,0:T(8,128)(2,1)} %shard_map.223), calls=%async_computation | async-start | bytes 1048576 | tf_op jit(solution)/shard_map/all_to_all | solution.py:30
  16.0 3.4 %shard_map.224 = bf16[64,48,128]{2,1,0:T(8,128)(2,1)} custom-call(s32[2,128]{1,0:T(2,128)} %bitcast.81, f32[2,128]{1,0:T(2,128)} %bitcast.79, bf16[128,512]{1,0:T(8,128)(2,1)} %refs_1_.6, bf16[128,1024]{1,0:T(8,128)(2,1)} %refs_0_.3, bf16[64,128]{1,0:T(8,128)(2,1)} %bitcast.71, f32[16,128]{1,0:T(8,128)} %bitcast.75, f32[1,16]{1,0:T(1,128)} %bitcast.85), custom_call_target="tpu_custom_call" | custom-call | flops 1073741824 | bytes 2097152 | tf_op jit(solution)/shard_map/pallas_call | solution.py:519
  19.4 14.3 %all-to-all-done = bf16[64,32,128]{2,1,0:T(8,128)(2,1)S(1)} async-done(((bf16[64,32,128]{2,1,0:T(8,128)(2,1)}), bf16[64,32,128]{2,1,0:T(8,128)(2,1)S(1)}, u32[]{:S(2)}, u32[]{:S(2)}) %all-to-all-start) | async-done | bytes 524320 | tf_op jit(solution)/shard_map/all_to_all | solution.py:30
  33.7 5.7 %all-to-all-start.1 = ((bf16[64,48,128]{2,1,0:T(8,128)(2,1)}), bf16[64,48,128]{2,1,0:T(8,128)(2,1)S(1)}, u32[]{:S(2)}, u32[]{:S(2)}) async-start(bf16[64,48,128]{2,1,0:T(8,128)(2,1)} %shard_map.224), calls=%async_computation.1 | async-start | bytes 1572864 | tf_op jit(solution)/shard_map/all_to_all | solution.py:30
  43.7 18.7 %all-to-all-done.1.got_ref = bf16[64,48,128]{2,1,0:T(8,128)(2,1)S(1)} async-done(((bf16[64,48,128]{2,1,0:T(8,128)(2,1)}), bf16[64,48,128]{2,1,0:T(8,128)(2,1)S(1)}, u32[]{:S(2)}, u32[]{:S(2)}) %all-to-all-start.1) | async-done | bytes 786464 | tf_op jit(solution)/shard_map/all_to_all | solution.py:30
  67.5 6.7 %all-to-all-start.2 = ((bf16[64,8,128]{2,1,0:T(8,128)(2,1)}), bf16[64,8,128]{2,1,0:T(8,128)(2,1)S(1)}, u32[]{:S(2)}, u32[]{:S(2)}) async-start(bf16[64,8,128]{2,1,0:T(8,128)(2,1)} %copy-done.5), calls=%async_computation.2 | async-start | bytes 262144 | tf_op jit(solution)/shard_map/all_to_all | solution.py:30
  74.3 4.1 %shard_map.225 = (f32[512,256]{1,0:T(8,128)}, f32[512,256]{1,0:T(8,128)}) custom-call(s32[1]{0:T(128)} %bitcast.refs_0_, bf16[512,512]{1,0:T(8,128)(2,1)S(1)} %bitcast.56, bf16[512,512]{1,0:T(8,128)(2,1)S(1)} %collective-permute-done.refs_2_, bf16[512,512]{1,0:T(8,128)(2,1)S(1)} %collective-permute-done.1.refs_3_, ...), custom_call_target="tpu_custom_call" | custom-call | flops 1073741824 | bytes 2097152 | tf_op jit(solution)/shard_map/pallas_call | solution.py:519
  78.5 10.3 %collective-permute-done.5.refs_4_.refs_8_ = bf16[512,512]{1,0:T(8,128)(2,1)} collective-permute-done((bf16[512,512]{1,0:T(8,128)(2,1)S(1)}, bf16[512,512]{1,0:T(8,128)(2,1)}, u32[]{:S(2)}, u32[]{:S(2)}) %collective-permute-start.5) | collective-permute-done | bytes 524320 | tf_op jit(solution)/shard_map/ppermute | solution.py:22
  88.8 7.3 %shard_map.226 = (bf16[512,256]{1,0:T(8,128)(2,1)}, bf16[512,256]{1,0:T(8,128)(2,1)}, bf16[512,256]{1,0:T(8,128)(2,1)}, bf16[512,512]{1,0:T(8,128)(2,1)}, bf16[5...) custom-call(s32[1]{0:T(128)} %bitcast.refs_0_, ...), custom_call_target="tpu_custom_call" | custom-call | flops 1073741824 | bytes 2097152 | tf_op jit(solution)/shard_map/pallas_call | solution.py:519
  98.9 3.5 %shard_map.229 = (bf16[128,1024]{1,0:T(8,128)(2,1)S(1)}, f32[128,1024]{1,0:T(8,128)}, bf16[64,1024]{1,0:T(8,128)(2,1)}, f32[128,1024]{1,0:T(8,128)}) custom-call(bf16[128,1024]{1,0:T(8,128)(2,1)} %refs_0_.3, bf16[128,1024]{1,0:T(8,128)(2,1)} %refs_3_.3, bf16[64,128]{1,0:T(8,128)(2,1)} %bitcast.72, bf16[64,128]{1,0:T(8,128)(2,1)} %bitcast.66, ...), custom_call_target="tpu_custom_call" | custom-call | flops 1073741824 | bytes 2097152 | tf_op jit(solution)/shard_map/pallas_call | solution.py:519
  103.5 3.5 %all-to-all-start.3 = ((bf16[4,128,1024]{2,1,0:T(8,128)(2,1)}), bf16[4,128,1024]{2,1,0:T(8,128)(2,1)S(1)}, u32[]{:S(2)}, u32[]{:S(2)}) async-start(bf16[4,128,1024]{2,1,0:T(8,128)(2,1)} %broadcast_in_dim.34), calls=%async_computation.3 | async-start | bytes 2097152 | tf_op jit(solution)/shard_map/all_to_all | solution.py:30
  111.4 9.0 %collective-permute-done.6 = bf16[512,512]{1,0:T(8,128)(2,1)} collective-permute-done((bf16[512,512]{1,0:T(8,128)(2,1)}, bf16[512,512]{1,0:T(8,128)(2,1)}, u32[]{:S(2)}, u32[]{:S(2)}) %collective-permute-start.6) | collective-permute-done | bytes 524320 | tf_op jit(solution)/shard_map/ppermute | solution.py:22
  122.0 31.5 %all_to_all.40 = bf16[64,8,512]{2,1,0:T(8,128)(2,1)S(1)} all-to-all(bf16[64,8,512]{2,1,0:T(8,128)(2,1)S(1)} %bitcast.63), channel_id=1, replica_groups=mesh['z'=8,'y'=4,'c'=2,'x'=4] {'z','y','c'}, dimensions={0} | all-to-all | bytes 1048576 | tf_op jit(solution)/shard_map/all_to_all | solution.py:30
  155.7 3.5 %all-to-all-start.5 = ((bf16[4,128,512]{2,1,0:T(8,128)(2,1)}), bf16[4,128,512]{2,1,0:T(8,128)(2,1)S(1)}, u32[]{:S(2)}, u32[]{:S(2)}) async-start(bf16[4,128,512]{2,1,0:T(8,128)(2,1)} %shard_map.230), calls=%async_computation.5 | async-start | bytes 1048576 | tf_op jit(solution)/shard_map/all_to_all | solution.py:30
  159.7 8.7 %all-to-all-done.5.refs_0_ = bf16[4,128,512]{2,1,0:T(8,128)(2,1)S(1)} async-done(((bf16[4,128,512]{2,1,0:T(8,128)(2,1)}), bf16[4,128,512]{2,1,0:T(8,128)(2,1)S(1)}, u32[]{:S(2)}, u32[]{:S(2)}) %all-to-all-start.5) | async-done | bytes 524320 | tf_op jit(solution)/shard_map/all_to_all | solution.py:30
  172.5 4.6 %shard_map.232 = (bf16[64,8,128]{2,1,0:T(8,128)(2,1)}, bf16[128,1024]{1,0:T(8,128)(2,1)}, f32[128,1024]{1,0:T(8,128)}) custom-call(bf16[4,128,512]{2,1,0:T(8,128)(2,1)S(1)} %all-to-all-done.5.refs_0_, bf16[2048,1024]{1,0:T(8,128)(2,1)} %refs_1_.7, f32[128,1024]{1,0:T(8,128)} %get-tuple-element.71.refs_2_, bf16[128,1024]{1,0:T(8,128)(2,1)} %refs_3_.3, ...), custom_call_target="tpu_custom_call" | custom-call | flops 1073741824 | bytes 2097152 | tf_op jit(solution)/shard_map/pallas_call | solution.py:519
  177.1 5.1 %all-to-all-start.6 = ((bf16[64,8,128]{2,1,0:T(8,128)(2,1)}), bf16[64,8,128]{2,1,0:T(8,128)(2,1)S(1)}, u32[]{:S(2)}, u32[]{:S(2)}) async-start(bf16[64,8,128]{2,1,0:T(8,128)(2,1)} %get-tuple-element.73), calls=%async_computation.6 | async-start | bytes 262144 | tf_op jit(solution)/shard_map/all_to_all | solution.py:30
  188.4 5.8 %shard_map.227 = (bf16[2048,256]{1,0:T(8,128)(2,1)}, bf16[2048,256]{1,0:T(8,128)(2,1)}, bf16[256,2048]{1,0:T(8,128)(2,1)}) custom-call(s32[1]{0:T(128)} %bitcast.refs_0_, bf16[512,512]{1,0:T(8,128)(2,1)} %bitcast.57, bf16[512,512]{1,0:T(8,128)(2,1)} %copy-done.2, bf16[512,512]{1,0:T(8,128)(2,1)} %copy-done.3, bf16[512,512]{1,0:T(8,128)(2,1)} %copy-done.4, ...), custom_call_target="tpu_custom_call" | custom-call | flops 4294967296 | bytes 2097152 | tf_op jit(solution)/shard_map/pallas_call | solution.py:519
  200.2 9.0 %all-to-all-start.7 = ((bf16[64,8,128]{2,1,0:T(8,128)(2,1)}), bf16[64,8,128]{2,1,0:T(8,128)(2,1)S(1)}, u32[]{:S(2)}, u32[]{:S(2)}) async-start(bf16[64,8,128]{2,1,0:T(8,128)(2,1)} %shard_map.233), calls=%async_computation.7 | async-start | bytes 262144 | tf_op jit(solution)/shard_map/all_to_all | solution.py:30
  209.2 3.8 %collective-permute-start.18 = (bf16[32,1024]{1,0:T(8,128)(2,1)S(1)}, bf16[32,1024]{1,0:T(8,128)(2,1)S(1)}, u32[]{:S(2)}, u32[]{:S(2)}) collective-permute-start(bf16[32,1024]{1,0:T(8,128)(2,1)S(1)} %get-tuple-element.68), channel_id=1, source_target_pairs={{0,192},{32,224},{64,0},{96,32},{128,64},{160,96},{192,128},{224,1... | collective-permute-start | bytes 196616 | tf_op jit(solution)/shard_map/ppermute | solution.py:22
  212.9 3.2 %collective-permute-start.16 = (bf16[32,1024]{1,0:T(8,128)(2,1)S(1)}, bf16[32,1024]{1,0:T(8,128)(2,1)S(1)}, u32[]{:S(2)}, u32[]{:S(2)}) collective-permute-start(bf16[32,1024]{1,0:T(8,128)(2,1)S(1)} %get-tuple-element.66), channel_id=1, source_target_pairs={{0,160},{32,192},{64,224},{96,0},{128,32},{160,64},{192,96},{224,1... | collective-permute-start | bytes 196616 | tf_op jit(solution)/shard_map/ppermute | solution.py:22
  216.2 4.1 %collective-permute-start.14 = (bf16[32,1024]{1,0:T(8,128)(2,1)S(1)}, bf16[32,1024]{1,0:T(8,128)(2,1)S(1)}, u32[]{:S(2)}, u32[]{:S(2)}) collective-permute-start(bf16[32,1024]{1,0:T(8,128)(2,1)S(1)} %get-tuple-element.64), channel_id=1, source_target_pairs={{0,128},{32,160},{64,192},{96,224},{128,0},{160,32},{192,64},{224,... | collective-permute-start | bytes 196616 | tf_op jit(solution)/shard_map/ppermute | solution.py:22
  220.2 5.4 %shard_map.234 = (f32[128,1024]{1,0:T(8,128)}, f32[128,1024]{1,0:T(8,128)}, f32[128,1024]{1,0:T(8,128)}, bf16[128,1024]{1,0:T(8,128)(2,1)}, f32[64,128]{1,0:T(8,...) custom-call(bf16[128,1024]{1,0:T(8,128)(2,1)} %refs_0_.3, bf16[64,128]{1,0:T(8,128)(2,1)} %bitcast.73, ...), custom_call_target="tpu_custom_call" | custom-call | flops 4294967296 | bytes 2097152 | tf_op jit(solution)/shard_map/pallas_call | solution.py:519
  226.4 3.7 %shard_map.235 = (bf16[128,1024]{1,0:T(8,128)(2,1)}, f32[64,128]{1,0:T(8,128)}, f32[16,128]{1,0:T(8,128)}) custom-call(bf16[64,8,128]{2,1,0:T(8,128)(2,1)S(1)} %all-to-all-done.7.refs_0_, bf16[64,1024]{1,0:T(8,128)(2,1)} %get-tuple-element.74.refs_6_.refs_1_, bf16[64,128]{1,0:T(8,128)(2,1)} %bitcast.74, f32[16,128]{1,0:T(8,128)} %bitcast.78, ...), custom_call_target="tpu_custom_call" | custom-call | flops 1073741824 | bytes 2097152 | tf_op jit(solution)/shard_map/pallas_call | solution.py:519
  (68 shorter events, 41.1 us)
Async XLA Ops:
  2.8 30.9 %all-to-all-start = ((bf16[64,32,128]{2,1,0:T(8,128)(2,1)}), bf16[64,32,128]{2,1,0:T(8,128)(2,1)S(1)}, u32[]{:S(2)}, u32[]{:S(2)}) async-start(bf16[64,32,128]{2,1,0:T(8,128)(2,1)} %shard_map.223), calls=%async_computation | async-start | bytes 1048576 | tf_op jit(solution)/shard_map/all_to_all | solution.py:30
  33.7 28.7 %all-to-all-start.1 = ((bf16[64,48,128]{2,1,0:T(8,128)(2,1)}), bf16[64,48,128]{2,1,0:T(8,128)(2,1)S(1)}, u32[]{:S(2)}, u32[]{:S(2)}) async-start(bf16[64,48,128]{2,1,0:T(8,128)(2,1)} %shard_map.224), calls=%async_computation.1 | async-start | bytes 1572864 | tf_op jit(solution)/shard_map/all_to_all | solution.py:30
  39.4 25.8 %collective-permute-start = (bf16[512,512]{1,0:T(8,128)(2,1)S(1)}, bf16[512,512]{1,0:T(8,128)(2,1)S(1)}, u32[]{:S(2)}, u32[]{:S(2)}) collective-permute-start(bf16[512,512]{1,0:T(8,128)(2,1)S(1)} %bitcast.53), channel_id=1, source_target_pairs={{0,1},{1,2},{2,3},{3,0},{4,5},{5,6},{6,7},{7,4},{8,9},{9,10},{10,1... | collective-permute-start | bytes 1572872 | tf_op jit(solution)/shard_map/ppermute | solution.py:22
  40.6 33.6 %collective-permute-start.1 = (bf16[512,512]{1,0:T(8,128)(2,1)S(1)}, bf16[512,512]{1,0:T(8,128)(2,1)S(1)}, u32[]{:S(2)}, u32[]{:S(2)}) collective-permute-start(bf16[512,512]{1,0:T(8,128)(2,1)S(1)} %bitcast.54), channel_id=1, source_target_pairs={{0,3},{1,0},{2,1},{3,2},{4,7},{5,4},{6,5},{7,6},{8,11},{9,8},{10,9... | collective-permute-start | bytes 1572872 | tf_op jit(solution)/shard_map/ppermute | solution.py:22
  42.1 32.2 %collective-permute-start.2 = (bf16[512,512]{1,0:T(8,128)(2,1)S(1)}, bf16[512,512]{1,0:T(8,128)(2,1)S(1)}, u32[]{:S(2)}, u32[]{:S(2)}) collective-permute-start(bf16[512,512]{1,0:T(8,128)(2,1)S(1)} %bitcast.55), channel_id=1, source_target_pairs={{0,2},{1,3},{2,0},{3,1},{4,6},{5,7},{6,4},{7,5},{8,10},{9,11},{10,... | collective-permute-start | bytes 1572872 | tf_op jit(solution)/shard_map/ppermute | solution.py:22
  62.4 16.1 %collective-permute-start.3 = (bf16[512,512]{1,0:T(8,128)(2,1)S(1)}, bf16[512,512]{1,0:T(8,128)(2,1)}, u32[]{:S(2)}, u32[]{:S(2)}) collective-permute-start(bf16[512,512]{1,0:T(8,128)(2,1)S(1)} %slice_bitcast_fusion.refs_1_.refs_5_), channel_id=1, source_target_pairs={{0,1},{1,2},{2,3},{3,0},{4,5},{5,6},{6,7},{7,4},{8,9},{9,10},{10,1... | collective-permute-start | bytes 1572872 | tf_op jit(solution)/shard_map/ppermute | solution.py:22
  63.7 14.8 %collective-permute-start.4 = (bf16[512,512]{1,0:T(8,128)(2,1)S(1)}, bf16[512,512]{1,0:T(8,128)(2,1)}, u32[]{:S(2)}, u32[]{:S(2)}) collective-permute-start(bf16[512,512]{1,0:T(8,128)(2,1)S(1)} %slice_bitcast_fusion.refs_1_.refs_5_), channel_id=1, source_target_pairs={{0,3},{1,0},{2,1},{3,2},{4,7},{5,4},{6,5},{7,6},{8,11},{9,8},{10,9... | collective-permute-start | bytes 1572872 | tf_op jit(solution)/shard_map/ppermute | solution.py:22
  65.2 23.6 %collective-permute-start.5 = (bf16[512,512]{1,0:T(8,128)(2,1)S(1)}, bf16[512,512]{1,0:T(8,128)(2,1)}, u32[]{:S(2)}, u32[]{:S(2)}) collective-permute-start(bf16[512,512]{1,0:T(8,128)(2,1)S(1)} %slice_bitcast_fusion.refs_1_.refs_5_), channel_id=1, source_target_pairs={{0,2},{1,3},{2,0},{3,1},{4,6},{5,7},{6,4},{7,5},{8,10},{9,11},{10,... | collective-permute-start | bytes 1572872 | tf_op jit(solution)/shard_map/ppermute | solution.py:22
  67.5 31.4 %all-to-all-start.2 = ((bf16[64,8,128]{2,1,0:T(8,128)(2,1)}), bf16[64,8,128]{2,1,0:T(8,128)(2,1)S(1)}, u32[]{:S(2)}, u32[]{:S(2)}) async-start(bf16[64,8,128]{2,1,0:T(8,128)(2,1)} %copy-done.5), calls=%async_computation.2 | async-start | bytes 262144 | tf_op jit(solution)/shard_map/all_to_all | solution.py:30
  96.1 12.5 %collective-permute-start.8 = (bf16[512,512]{1,0:T(8,128)(2,1)}, bf16[512,512]{1,0:T(8,128)(2,1)S(1)}, u32[]{:S(2)}, u32[]{:S(2)}) collective-permute-start(bf16[512,512]{1,0:T(8,128)(2,1)} %get-tuple-element.59), channel_id=1, source_target_pairs={{0,3},{1,0},{2,1},{3,2},{4,7},{5,4},{6,5},{7,6},{8,11},{9,8},{10,9... | collective-permute-start | bytes 1572872 | tf_op jit(solution)/shard_map/ppermute | solution.py:22
  97.6 13.8 %collective-permute-start.7 = (bf16[512,512]{1,0:T(8,128)(2,1)}, bf16[512,512]{1,0:T(8,128)(2,1)}, u32[]{:S(2)}, u32[]{:S(2)}) collective-permute-start(bf16[512,512]{1,0:T(8,128)(2,1)} %get-tuple-element.58), channel_id=1, source_target_pairs={{0,1},{1,2},{2,3},{3,0},{4,5},{5,6},{6,7},{7,4},{8,9},{9,10},{10,1... | collective-permute-start | bytes 1572872 | tf_op jit(solution)/shard_map/ppermute | solution.py:22
  97.9 22.5 %collective-permute-start.6 = (bf16[512,512]{1,0:T(8,128)(2,1)}, bf16[512,512]{1,0:T(8,128)(2,1)}, u32[]{:S(2)}, u32[]{:S(2)}) collective-permute-start(bf16[512,512]{1,0:T(8,128)(2,1)} %get-tuple-element.57), channel_id=1, source_target_pairs={{0,2},{1,3},{2,0},{3,1},{4,6},{5,7},{6,4},{7,5},{8,10},{9,11},{10,... | collective-permute-start | bytes 1572872 | tf_op jit(solution)/shard_map/ppermute | solution.py:22
  103.5 18.5 %all-to-all-start.3 = ((bf16[4,128,1024]{2,1,0:T(8,128)(2,1)}), bf16[4,128,1024]{2,1,0:T(8,128)(2,1)S(1)}, u32[]{:S(2)}, u32[]{:S(2)}) async-start(bf16[4,128,1024]{2,1,0:T(8,128)(2,1)} %broadcast_in_dim.34), calls=%async_computation.3 | async-start | bytes 2097152 | tf_op jit(solution)/shard_map/all_to_all | solution.py:30
  155.7 12.6 %all-to-all-start.5 = ((bf16[4,128,512]{2,1,0:T(8,128)(2,1)}), bf16[4,128,512]{2,1,0:T(8,128)(2,1)S(1)}, u32[]{:S(2)}, u32[]{:S(2)}) async-start(bf16[4,128,512]{2,1,0:T(8,128)(2,1)} %shard_map.230), calls=%async_computation.5 | async-start | bytes 1048576 | tf_op jit(solution)/shard_map/all_to_all | solution.py:30
  159.2 35.0 %collective-permute-start.13 = (bf16[4,128,1024]{2,1,0:T(8,128)(2,1)S(1)}, bf16[4,128,1024]{2,1,0:T(8,128)(2,1)S(1)}, u32[]{:S(2)}, u32[]{:S(2)}) collective-permute-start(bf16[4,128,1024]{2,1,0:T(8,128)(2,1)S(1)} %all-to-all-done.3.refs_5_), channel_id=1, source_target_pairs={{0,4},{4,0},{1,5},{5,1},{2,6},{6,2},{3,7},{7,3},{8,12},{12,8},{9,1... | collective-permute-start | bytes 3145736 | tf_op jit(solution)/shard_map/ppermute | solution.py:22
  171.2 11.0 %collective-permute-start.9 = (bf16[4,8,32,128]{3,2,0,1:T(8,128)(2,1)}, bf16[4,8,32,128]{3,2,0,1:T(8,128)(2,1)}, u32[]{:S(2)}, u32[]{:S(2)}) collective-permute-start(bf16[4,8,32,128]{3,2,0,1:T(8,128)(2,1)} %get-tuple-element.91), channel_id=1, source_target_pairs={{0,4},{4,0},{1,5},{5,1},{2,6},{6,2},{3,7},{7,3},{8,12},{12,8},{9,1... | collective-permute-start | bytes 786440 | tf_op jit(solution)/shard_map/ppermute | solution.py:22
  177.1 22.2 %all-to-all-start.6 = ((bf16[64,8,128]{2,1,0:T(8,128)(2,1)}), bf16[64,8,128]{2,1,0:T(8,128)(2,1)S(1)}, u32[]{:S(2)}, u32[]{:S(2)}) async-start(bf16[64,8,128]{2,1,0:T(8,128)(2,1)} %get-tuple-element.73), calls=%async_computation.6 | async-start | bytes 262144 | tf_op jit(solution)/shard_map/all_to_all | solution.py:30
  183.3 10.8 %collective-permute-start.10 = (bf16[2,8,32,128]{3,2,1,0:T(8,128)(2,1)S(1)}, bf16[2,8,32,128]{3,2,1,0:T(8,128)(2,1)S(1)}, u32[]{:S(2)}, u32[]{:S(2)}) collective-permute-start(bf16[2,8,32,128]{3,2,1,0:T(8,128)(2,1)S(1)} %get-tuple-element.89), channel_id=1, source_target_pairs={{0,8},{8,16},{16,24},{24,0},{1,9},{9,17},{17,25},{25,1},{2,10},{10... | collective-permute-start | bytes 393224 | tf_op jit(solution)/shard_map/ppermute | solution.py:22
  197.0 19.2 %collective-permute-start.20 = (bf16[32,1024]{1,0:T(8,128)(2,1)}, bf16[32,1024]{1,0:T(8,128)(2,1)S(1)}, u32[]{:S(2)}, u32[]{:S(2)}) collective-permute-start(bf16[32,1024]{1,0:T(8,128)(2,1)} %get-tuple-element.70), channel_id=1, source_target_pairs={{0,224},{32,0},{64,32},{96,64},{128,96},{160,128},{192,160},{224,1... | collective-permute-start | bytes 196616 | tf_op jit(solution)/shard_map/ppermute | solution.py:22
  199.3 16.8 %collective-permute-start.19 = (bf16[32,1024]{1,0:T(8,128)(2,1)S(1)}, bf16[32,1024]{1,0:T(8,128)(2,1)S(1)}, u32[]{:S(2)}, u32[]{:S(2)}) collective-permute-start(bf16[32,1024]{1,0:T(8,128)(2,1)S(1)} %get-tuple-element.69), channel_id=1, source_target_pairs={{0,32},{32,64},{64,96},{96,128},{128,160},{160,192},{192,224},{224... | collective-permute-start | bytes 196616 | tf_op jit(solution)/shard_map/ppermute | solution.py:22
  200.2 26.2 %all-to-all-start.7 = ((bf16[64,8,128]{2,1,0:T(8,128)(2,1)}), bf16[64,8,128]{2,1,0:T(8,128)(2,1)S(1)}, u32[]{:S(2)}, u32[]{:S(2)}) async-start(bf16[64,8,128]{2,1,0:T(8,128)(2,1)} %shard_map.233), calls=%async_computation.7 | async-start | bytes 262144 | tf_op jit(solution)/shard_map/all_to_all | solution.py:30
  209.2 16.4 %collective-permute-start.18 = (bf16[32,1024]{1,0:T(8,128)(2,1)S(1)}, bf16[32,1024]{1,0:T(8,128)(2,1)S(1)}, u32[]{:S(2)}, u32[]{:S(2)}) collective-permute-start(bf16[32,1024]{1,0:T(8,128)(2,1)S(1)} %get-tuple-element.68), channel_id=1, source_target_pairs={{0,192},{32,224},{64,0},{96,32},{128,64},{160,96},{192,128},{224,1... | collective-permute-start | bytes 196616 | tf_op jit(solution)/shard_map/ppermute | solution.py:22
  212.9 12.7 %collective-permute-start.17 = (bf16[32,1024]{1,0:T(8,128)(2,1)S(1)}, bf16[32,1024]{1,0:T(8,128)(2,1)S(1)}, u32[]{:S(2)}, u32[]{:S(2)}) collective-permute-start(bf16[32,1024]{1,0:T(8,128)(2,1)S(1)} %get-tuple-element.67), channel_id=1, source_target_pairs={{0,64},{32,96},{64,128},{96,160},{128,192},{160,224},{192,0},{224,... | collective-permute-start | bytes 196616 | tf_op jit(solution)/shard_map/ppermute | solution.py:22
  212.9 12.7 %collective-permute-start.16 = (bf16[32,1024]{1,0:T(8,128)(2,1)S(1)}, bf16[32,1024]{1,0:T(8,128)(2,1)S(1)}, u32[]{:S(2)}, u32[]{:S(2)}) collective-permute-start(bf16[32,1024]{1,0:T(8,128)(2,1)S(1)} %get-tuple-element.66), channel_id=1, source_target_pairs={{0,160},{32,192},{64,224},{96,0},{128,32},{160,64},{192,96},{224,1... | collective-permute-start | bytes 196616 | tf_op jit(solution)/shard_map/ppermute | solution.py:22
  (11 other events, 176.7 us)
where the time goes:
time: 233 us; the launch traced here: 230 us
  starting transfers between devices  78.1 us (34%)
  waiting for transfers between devices  65.8 us (28%)
  Pallas kernels  45.5 us (20%)
  blocking collectives  31.5 us (14%)
  local copies, waits for them, and re-layouts  4.68 us (2%)
  other arithmetic  3.56 us (2%)
    all_to_all x7, starting transfers between devices, to_all(): return lax.all_to_all(value, axes, split_axis=0, concat_axis=0, tiled=True)  46.6 us
    pallas_call x13, Pallas kernels, local(): found = call(*arrays)  45.5 us
    all_to_all x7, waiting for transfers between devices, to_all(): return lax.all_to_all(value, axes, split_axis=0, concat_axis=0, tiled=True)  41.7 us
    ppermute x21, starting transfers between devices, along(): lax.ppermute(value, axis, [(i, (i + step) % count) for i in range(count)])  31.5 us
    all_to_all x1, blocking collectives, to_all(): return lax.all_to_all(value, axes, split_axis=0, concat_axis=0, tiled=True)  31.5 us
    ppermute x21, waiting for transfers between devices, along(): lax.ppermute(value, axis, [(i, (i + step) % count) for i in range(count)])  24.1 us
  transfers between devices with their start and end apart: 28, of which 8 were waited for; matrix products, arithmetic and copies ran while one was open for 3% of the time, Pallas kernels for 16%

commit v1 on v0

--- a/solution.py
+++ b/solution.py
@@ -41,6 +41,29 @@
 
 
 SMALL, LARGE = 1 << 30, 1 << 32
+
+
+def staged_kernel(*refs):
+    half = len(refs) // 2
+    copies = [
+        pltpu.make_async_copy(source, target, refs[-1].at[k])
+        for k, (source, target) in enumerate(zip(refs[:half], refs[half:-1]))
+    ]
+    for copy in copies:
+        copy.start()
+    for copy in copies:
+        copy.wait()
+
+
+def staged(arrays):
+    return pl.pallas_call(
+        staged_kernel,
+        out_shape=tuple(pltpu.VMEM(a.shape, a.dtype) for a in arrays),
+        in_specs=[pl.BlockSpec(memory_space=pltpu.HBM)] * len(arrays),
+        scratch_shapes=(pltpu.SemaphoreType.DMA((len(arrays),)),),
+        compiler_params=pltpu.CompilerParams(vmem_limit_bytes=16 << 20),
+        cost_estimate=pl.CostEstimate(flops=SMALL, bytes_accessed=1 << 22, transcendentals=0),
+    )(*[pltpu.with_memory_space_constraint(a, pltpu.HBM) for a in arrays])
 
 
 def softplus(value):
@@ -222,9 +245,9 @@
         out_ref[...] = total
 
 
-def middle_kernel(
+def hidden_kernel(
     here_ref, own_ref, left_ref, right_ref, op_ref, down_ref, pre_ref, up_pre_ref, gate_ref, up_ref,
-    hidden_ref, gate_grad_ref, up_grad_ref, far_ref, next_ref, back_ref, rest_ref,
+    hidden_ref, gate_grad_ref, up_grad_ref, term_ref,
 ):
     here = here_ref[0]
     hidden_grad = None
@@ -241,13 +264,31 @@
     up_grad = (hidden_grad * active).astype(BF16)
     gate_grad_ref[...] = gate_grad
     up_grad_ref[...] = up_grad
+    width = term_ref.shape[1]
+    at = pl.multiple_of(((here + 2) & 3) * width, width)
+    term_ref[...] = (
+        mm_nt(gate_grad, gate_ref[pl.ds(at, width), :]) + mm_nt(up_grad, up_ref[pl.ds(at, width), :])
+    ).astype(BF16)
+
+
+def terms_kernel(
+    here_ref, gate_grad_ref, up_grad_ref, gate_ref, up_ref, next_ref, back_ref, rest_ref
+):
+    here = here_ref[0]
+    gate_grad, up_grad = gate_grad_ref[...], up_grad_ref[...]
     width = rest_ref.shape[1]
-    for offset, term_ref in ((2, far_ref), (1, next_ref), (3, back_ref), (0, rest_ref)):
+    for offset, term_ref in ((1, next_ref), (3, back_ref), (0, rest_ref)):
         at = pl.multiple_of(((here + offset) & 3) * width, width)
         term = mm_nt(gate_grad, gate_ref[pl.ds(at, width), :]) + mm_nt(
             up_grad, up_ref[pl.ds(at, width), :]
         )
         term_ref[...] = term.astype(BF16)
+
+
+def sum_kernel(own_ref, left_ref, right_ref, far_ref, out_ref):
+    total = own_ref[...].astype(F32) + left_ref[...].astype(F32)
+    total = total + right_ref[...].astype(F32) + far_ref[...].astype(F32)
+    out_ref[...] = total.astype(BF16)
 
 
 def weights_kernel(
@@ -337,6 +378,8 @@
     gated = mixed * z_act
     scale = lax.rsqrt(jnp.mean(gated * gated, axis=1, keepdims=True) + EPS)
     rows = jnp.concatenate([rows_ref[k] for k in range(rows_ref.shape[0])], axis=1)
+    w_ref, arrived = w_ref
+    arrived.wait()
     d_norm = mm(rows, w_ref[...]) * gain_ref[...]
     along_row = jnp.mean(d_norm * gated, axis=1, keepdims=True)
     d_gated = scale * d_norm - gated * (scale * scale * scale * along_row)
@@ -475,14 +518,15 @@
 
 
 class Held:
-    def __init__(self, array):
-        self.array = array
+    def __init__(self, array, late=False):
+        self.array, self.late = array, late
 
 
 def local(kernel, outs, args, flops, scratch=(), scalars=0, away=()):
     outs = outs if isinstance(outs, tuple) else (outs,)
     outs = tuple(pltpu.HBM(o.shape, o.dtype) if i in away else o for i, o in enumerate(outs))
     held = [i for i, a in enumerate(args) if isinstance(a, Held)]
+    held.sort(key=lambda i: args[i].late)
     arrays = [
         pltpu.with_memory_space_constraint(a.array, pltpu.HBM) if isinstance(a, Held) else a
         for a in args
@@ -497,9 +541,13 @@
         refs, inside, sems = list(refs[:count]), refs[count:-1], refs[-1]
         copies = []
         for k, i in enumerate(held):
-            copies.append(pltpu.make_async_copy(refs[i], inside[k], sems.at[k]))
-            copies[-1].start()
-            refs[i] = inside[k]
+            copy = pltpu.make_async_copy(refs[i], inside[k], sems.at[k])
+            copy.start()
+            if args[i].late:
+                refs[i] = (inside[k], copy)
+            else:
+                refs[i] = inside[k]
+                copies.append(copy)
         for copy in copies:
             copy.wait()
         kernel(*refs)
@@ -578,24 +626,37 @@
     pieces = local(ahead_kernel, shape((experts, 8, LANES), BF16), (got_grad,), SMALL)
     pieces = to_all(pieces, SP)
 
-    hidden, gate_grad, up_grad, term_far, term_next, term_back, term_own = local(
-        middle_kernel,
+    down_near, gate_near, up_near, pre_near, up_pre_near = staged(
+        (down_w, gate_w, up_w, pre, up_pre)
+    )
+    hidden, gate_grad, up_grad, term_far = local(
+        hidden_kernel,
         (
             shape((slots, inner), BF16),
             shape((slots, inner), BF16),
             shape((slots, inner), BF16),
-            *[shape((slots, cols), BF16)] * 4,
-        ),
-        (here, rows_grad, grad_left, grad_right, grad_far, Held(down_w), Held(pre), Held(up_pre), Held(gate_w), Held(up_w)),
+            shape((slots, cols), BF16),
+        ),
+        (
+            here, rows_grad, grad_left, grad_right, grad_far, down_near, pre_near, up_pre_near,
+            gate_near, up_near,
+        ),
         SMALL,
         scalars=1,
-        away=(0, 1, 2),
-    )
-    terms = shifted(term_far, 2), shifted(term_next, 1), shifted(term_back, -1)
-    slot_grad = term_own.astype(F32)
-    for term in terms:
-        slot_grad = slot_grad + term.astype(F32)
-    slot_grad = slot_grad.astype(BF16)
+        away=(0,),
+    )
+    term_far = shifted(term_far, 2)
+    term_next, term_back, term_own = local(
+        terms_kernel,
+        (shape((slots, cols), BF16), shape((slots, cols), BF16), shape((slots, cols), BF16)),
+        (here, gate_grad, up_grad, gate_near, up_near),
+        SMALL,
+        scalars=1,
+        away=(2,),
+    )
+    terms = shifted(term_next, 1), shifted(term_back, -1)
+    own_near = staged((term_own,))[0]
+    slot_grad = local(sum_kernel, shape((slots, cols), BF16), (own_near, *terms, term_far), SMALL)
 
     norm_rows, mixed, start_state, start_wide = local(
         forward_kernel,
@@ -641,6 +702,7 @@
         SMALL,
     )
     mixer4 = to_all(mixer_cols, "x")
+    mixed_near, wide_near = staged((mixed, start_wide))
 
     pieces, grad_z, d_mixed = local(
         gate_back_kernel,
@@ -649,7 +711,7 @@
             shape((tok, wide), BF16),
             shape((tok, wide), F32),
         ),
-        (mixer4, Held(w_out), Held(mixed), Held(gate_z), Held(gain), Held(start_wide), Held(c_t)),
+        (mixer4, Held(w_out, True), mixed_near, Held(gate_z), Held(gain), wide_near, Held(c_t)),
         SMALL,
         away=(2,),
     )

time: 233 us -> 232 us (level)
  starting transfers between devices: 78.1 us -> 83.2 us
  blocking collectives: 31.5 us -> 26.6 us
  other arithmetic: 3.56 us -> 0.86 us
    all_to_all x1, blocking collectives: 31.5 us -> 26.6 us  [to_all(): return lax.all_to_all(value, axes, split_axis=0, concat_axis=0, tiled=True)]
    pallas_call x0 -> x3, Pallas kernels: none -> 4.46 us  [staged(): pl.pallas_call(staged_kernel, out_shape=tuple((pltpu.VMEM(a.shape, a.dtyp...]
    unnamed x14 -> x24, local copies, waits for them, and re-layouts: 0.67 us -> 5.06 us
    ppermute x21, starting transfers between devices: 31.5 us -> 35.3 us  [along(): lax.ppermute(value, axis, [(i, (i + step) % count) for i in range(count)])]
    ppermute x21, waiting for transfers between devices: 24.1 us -> 21.3 us  [along(): lax.ppermute(value, axis, [(i, (i + step) % count) for i in range(count)])]
    pallas_call x13 -> x15, Pallas kernels: 45.5 us -> 43 us  [local(): found = call(*arrays)]
  transfers between devices with their start and end apart: 28 -> 28, of which waited for: 8 -> 7; matrix products, arithmetic and copies ran while one was open for 3% -> 1% of each run, Pallas kernels for 16% -> 17%
where the time goes in v1:
time: 232 us; the launch traced here: 231 us
  starting transfers between devices  83.2 us (36%)
  waiting for transfers between devices  65.3 us (28%)
  Pallas kernels  47.5 us (20%)
  blocking collectives  26.6 us (11%)
  local copies, waits for them, and re-layouts  6.5 us (3%)
    all_to_all x7, starting transfers between devices, to_all(): return lax.all_to_all(value, axes, split_axis=0, concat_axis=0, tiled=True)  47.9 us
    all_to_all x7, waiting for transfers between devices, to_all(): return lax.all_to_all(value, axes, split_axis=0, concat_axis=0, tiled=True)  44 us
    pallas_call x15, Pallas kernels, local(): found = call(*arrays)  43 us
    ppermute x21, starting transfers between devices, along(): lax.ppermute(value, axis, [(i, (i + step) % count) for i in range(count)])  35.3 us
    all_to_all x1, blocking collectives, to_all(): return lax.all_to_all(value, axes, split_axis=0, concat_axis=0, tiled=True)  26.6 us
    ppermute x21, waiting for transfers between devices, along(): lax.ppermute(value, axis, [(i, (i + step) % count) for i in range(count)])  21.3 us
    unnamed x24, local copies, waits for them, and re-layouts  5.06 us
  transfers between devices with their start and end apart: 28, of which 7 were waited for; matrix products, arithmetic and copies ran while one was open for 1% of the time, Pallas kernels for 17%

profile of v1, /device:TPU:1, one launch (start us, length us, event | category | flops | bytes accessed | tf_op | source)
XLA Modules:
  0.0 231.1 jit_solution(2973600194977563594)
XLA Ops:
  2.8 13.2 %all-to-all-start = ((bf16[64,32,128]{2,1,0:T(8,128)(2,1)}), bf16[64,32,128]{2,1,0:T(8,128)(2,1)S(1)}, u32[]{:S(2)}, u32[]{:S(2)}) async-start(bf16[64,32,128]{2,1,0:T(8,128)(2,1)} %shard_map.223), calls=%async_computation | async-start | bytes 1048576 | tf_op jit(solution)/shard_map/all_to_all | solution.py:30
  16.0 3.4 %shard_map.224 = bf16[64,48,128]{2,1,0:T(8,128)(2,1)} custom-call(s32[2,128]{1,0:T(2,128)} %bitcast.82, f32[2,128]{1,0:T(2,128)} %bitcast.80, bf16[128,512]{1,0:T(8,128)(2,1)} %refs_1_.6, bf16[128,1024]{1,0:T(8,128)(2,1)} %refs_0_.3, bf16[64,128]{1,0:T(8,128)(2,1)} %bitcast.72, f32[16,128]{1,0:T(8,128)} %bitcast.76, f32[1,16]{1,0:T(1,128)} %bitcast.86), custom_call_target="tpu_custom_call" | custom-call | flops 1073741824 | bytes 2097152 | tf_op jit(solution)/shard_map/pallas_call | solution.py:567
  19.4 14.3 %all-to-all-done = bf16[64,32,128]{2,1,0:T(8,128)(2,1)S(1)} async-done(((bf16[64,32,128]{2,1,0:T(8,128)(2,1)}), bf16[64,32,128]{2,1,0:T(8,128)(2,1)S(1)}, u32[]{:S(2)}, u32[]{:S(2)}) %all-to-all-start) | async-done | bytes 524320 | tf_op jit(solution)/shard_map/all_to_all | solution.py:30
  33.7 5.7 %all-to-all-start.1 = ((bf16[64,48,128]{2,1,0:T(8,128)(2,1)}), bf16[64,48,128]{2,1,0:T(8,128)(2,1)S(1)}, u32[]{:S(2)}, u32[]{:S(2)}) async-start(bf16[64,48,128]{2,1,0:T(8,128)(2,1)} %shard_map.224), calls=%async_computation.1 | async-start | bytes 1572864 | tf_op jit(solution)/shard_map/all_to_all | solution.py:30
  43.7 18.7 %all-to-all-done.1.got_ref = bf16[64,48,128]{2,1,0:T(8,128)(2,1)S(1)} async-done(((bf16[64,48,128]{2,1,0:T(8,128)(2,1)}), bf16[64,48,128]{2,1,0:T(8,128)(2,1)S(1)}, u32[]{:S(2)}, u32[]{:S(2)}) %all-to-all-start.1) | async-done | bytes 786464 | tf_op jit(solution)/shard_map/all_to_all | solution.py:30
  67.5 6.7 %all-to-all-start.2 = ((bf16[64,8,128]{2,1,0:T(8,128)(2,1)}), bf16[64,8,128]{2,1,0:T(8,128)(2,1)S(1)}, u32[]{:S(2)}, u32[]{:S(2)}) async-start(bf16[64,8,128]{2,1,0:T(8,128)(2,1)} %copy-done.9), calls=%async_computation.2 | async-start | bytes 262144 | tf_op jit(solution)/shard_map/all_to_all | solution.py:30
  74.3 4.1 %shard_map.225 = (f32[512,256]{1,0:T(8,128)}, f32[512,256]{1,0:T(8,128)}) custom-call(s32[1]{0:T(128)} %bitcast.refs_0_.here_ref, bf16[512,512]{1,0:T(8,128)(2,1)S(1)} %bitcast.56, bf16[512,512]{1,0:T(8,128)(2,1)S(1)} %collective-permute-done.refs_2_, bf16[512,512]{1,0:T(8,128)(2,1)S(1)} %collective-permute-done.1.refs_3_, ...), custom_call_target="tpu_custom_call" | custom-call | flops 1073741824 | bytes 2097152 | tf_op jit(solution)/shard_map/pallas_call | solution.py:567
  85.4 3.5 %shard_map.233 = (bf16[128,1024]{1,0:T(8,128)(2,1)S(1)}, f32[128,1024]{1,0:T(8,128)}, bf16[64,1024]{1,0:T(8,128)(2,1)}, f32[128,1024]{1,0:T(8,128)}) custom-call(bf16[128,1024]{1,0:T(8,128)(2,1)} %refs_0_.3, bf16[128,1024]{1,0:T(8,128)(2,1)} %refs_3_.3, bf16[64,128]{1,0:T(8,128)(2,1)} %bitcast.73, bf16[64,128]{1,0:T(8,128)(2,1)} %bitcast.67, ...), custom_call_target="tpu_custom_call" | custom-call | flops 1073741824 | bytes 2097152 | tf_op jit(solution)/shard_map/pallas_call | solution.py:567
  90.0 4.4 %all-to-all-start.3 = ((bf16[4,128,1024]{2,1,0:T(8,128)(2,1)}), bf16[4,128,1024]{2,1,0:T(8,128)(2,1)}, u32[]{:S(2)}, u32[]{:S(2)}) async-start(bf16[4,128,1024]{2,1,0:T(8,128)(2,1)} %broadcast_in_dim.34), calls=%async_computation.3 | async-start | bytes 2097152 | tf_op jit(solution)/shard_map/all_to_all | solution.py:30
  96.9 3.1 %shard_map.227 = (bf16[512,256]{1,0:T(8,128)(2,1)}, bf16[512,256]{1,0:T(8,128)(2,1)S(1)}, bf16[512,256]{1,0:T(8,128)(2,1)S(1)}, bf16[512,512]{1,0:T(8,128)(2,1)S(1)}) custom-call(s32[1]{0:T(128)} %bitcast.refs_0_.here_ref, bf16[512,512]{1,0:T(8,128)(2,1)S(1)} %slice_bitcast_fusion.own_ref.refs_5_, bf16[512,512]{1,0:T(8,128)(2,1)} %collective-permute-done.3.left_ref.refs_6_, ...), custom_call_target="tpu_custom_call" | custom-call | flops 1073741824 | bytes 2097152 | tf_op jit(solution)/shard_map/pallas_call | solution.py:567
  105.8 11.0 %collective-permute-done.6.left_ref = bf16[512,512]{1,0:T(8,128)(2,1)S(1)} collective-permute-done((bf16[512,512]{1,0:T(8,128)(2,1)S(1)}, bf16[512,512]{1,0:T(8,128)(2,1)S(1)}, u32[]{:S(2)}, u32[]{:S(2)}) %collective-permute-start.6) | collective-permute-done | bytes 524320 | tf_op jit(solution)/shard_map/ppermute | solution.py:22
  116.8 10.0 %collective-permute-done.8.far_ref = bf16[512,512]{1,0:T(8,128)(2,1)S(1)} collective-permute-done((bf16[512,512]{1,0:T(8,128)(2,1)S(1)}, bf16[512,512]{1,0:T(8,128)(2,1)S(1)}, u32[]{:S(2)}, u32[]{:S(2)}) %collective-permute-start.8) | collective-permute-done | bytes 524320 | tf_op jit(solution)/shard_map/ppermute | solution.py:22
  127.0 26.6 %all_to_all.40 = bf16[64,8,512]{2,1,0:T(8,128)(2,1)S(1)} all-to-all(bf16[64,8,512]{2,1,0:T(8,128)(2,1)S(1)} %bitcast.58), channel_id=1, replica_groups=mesh['z'=8,'y'=4,'c'=2,'x'=4] {'z','y','c'}, dimensions={0} | all-to-all | bytes 1048576 | tf_op jit(solution)/shard_map/all_to_all | solution.py:30
  155.8 3.9 %all-to-all-start.5 = ((bf16[4,128,512]{2,1,0:T(8,128)(2,1)}), bf16[4,128,512]{2,1,0:T(8,128)(2,1)S(1)}, u32[]{:S(2)}, u32[]{:S(2)}) async-start(bf16[4,128,512]{2,1,0:T(8,128)(2,1)} %shard_map.234), calls=%async_computation.5 | async-start | bytes 1048576 | tf_op jit(solution)/shard_map/all_to_all | solution.py:30
  160.4 8.2 %all-to-all-done.5.refs_0_ = bf16[4,128,512]{2,1,0:T(8,128)(2,1)S(1)} async-done(((bf16[4,128,512]{2,1,0:T(8,128)(2,1)}), bf16[4,128,512]{2,1,0:T(8,128)(2,1)S(1)}, u32[]{:S(2)}, u32[]{:S(2)}) %all-to-all-start.5) | async-done | bytes 524320 | tf_op jit(solution)/shard_map/all_to_all | solution.py:30
  171.9 4.2 %shard_map.237 = (bf16[64,8,128]{2,1,0:T(8,128)(2,1)}, bf16[128,1024]{1,0:T(8,128)(2,1)}, f32[128,1024]{1,0:T(8,128)}) custom-call(bf16[4,128,512]{2,1,0:T(8,128)(2,1)S(1)} %all-to-all-done.5.refs_0_, bf16[2048,1024]{1,0:T(8,128)(2,1)} %refs_1_.7, f32[128,1024]{1,0:T(8,128)S(1)} %get-tuple-element.85.refs_2_, bf16[128,1024]{1,0:T(8,128)(2,1)} %refs_3_.3, ...), custom_call_target="tpu_custom_call" | custom-call | flops 1073741824 | bytes 2097152 | tf_op jit(solution)/shard_map/pallas_call | solution.py:567
  176.1 5.1 %all-to-all-start.6 = ((bf16[64,8,128]{2,1,0:T(8,128)(2,1)}), bf16[64,8,128]{2,1,0:T(8,128)(2,1)S(1)}, u32[]{:S(2)}, u32[]{:S(2)}) async-start(bf16[64,8,128]{2,1,0:T(8,128)(2,1)} %get-tuple-element.87), calls=%async_computation.6 | async-start | bytes 262144 | tf_op jit(solution)/shard_map/all_to_all | solution.py:30
  186.3 5.8 %shard_map.228 = (bf16[2048,256]{1,0:T(8,128)(2,1)}, bf16[2048,256]{1,0:T(8,128)(2,1)}, bf16[256,2048]{1,0:T(8,128)(2,1)}) custom-call(s32[1]{0:T(128)} %bitcast.refs_0_.here_ref, bf16[512,512]{1,0:T(8,128)(2,1)} %bitcast.57, bf16[512,512]{1,0:T(8,128)(2,1)} %copy-done.6, bf16[512,512]{1,0:T(8,128)(2,1)} %copy-done.7, bf16[512,512]{1,0:T(8,128)(2,1)} %copy-done.8, ...), custom_call_target="tpu_custom_call" | custom-call | flops 4294967296 | bytes 2097152 | tf_op jit(solution)/shard_map/pallas_call | solution.py:567
  194.9 5.1 %collective-permute-start.14 = (bf16[32,1024]{1,0:T(8,128)(2,1)S(1)}, bf16[32,1024]{1,0:T(8,128)(2,1)S(1)}, u32[]{:S(2)}, u32[]{:S(2)}) collective-permute-start(bf16[32,1024]{1,0:T(8,128)(2,1)S(1)} %get-tuple-element.76), channel_id=1, source_target_pairs={{0,128},{32,160},{64,192},{96,224},{128,0},{160,32},{192,64},{224,... | collective-permute-start | bytes 196616 | tf_op jit(solution)/shard_map/ppermute | solution.py:22
  201.4 8.8 %all-to-all-start.7 = ((bf16[64,8,128]{2,1,0:T(8,128)(2,1)}), bf16[64,8,128]{2,1,0:T(8,128)(2,1)S(1)}, u32[]{:S(2)}, u32[]{:S(2)}) async-start(bf16[64,8,128]{2,1,0:T(8,128)(2,1)} %shard_map.238), calls=%async_computation.7 | async-start | bytes 262144 | tf_op jit(solution)/shard_map/all_to_all | solution.py:30
  210.2 4.6 %collective-permute-start.16 = (bf16[32,1024]{1,0:T(8,128)(2,1)S(1)}, bf16[32,1024]{1,0:T(8,128)(2,1)S(1)}, u32[]{:S(2)}, u32[]{:S(2)}) collective-permute-start(bf16[32,1024]{1,0:T(8,128)(2,1)S(1)} %get-tuple-element.78), channel_id=1, source_target_pairs={{0,160},{32,192},{64,224},{96,0},{128,32},{160,64},{192,96},{224,1... | collective-permute-start | bytes 196616 | tf_op jit(solution)/shard_map/ppermute | solution.py:22
  215.2 3.2 %collective-permute-start.18 = (bf16[32,1024]{1,0:T(8,128)(2,1)S(1)}, bf16[32,1024]{1,0:T(8,128)(2,1)S(1)}, u32[]{:S(2)}, u32[]{:S(2)}) collective-permute-start(bf16[32,1024]{1,0:T(8,128)(2,1)S(1)} %get-tuple-element.80), channel_id=1, source_target_pairs={{0,192},{32,224},{64,0},{96,32},{128,64},{160,96},{192,128},{224,1... | collective-permute-start | bytes 196616 | tf_op jit(solution)/shard_map/ppermute | solution.py:22
  221.1 5.3 %shard_map.239 = (f32[128,1024]{1,0:T(8,128)}, f32[128,1024]{1,0:T(8,128)}, f32[128,1024]{1,0:T(8,128)}, bf16[128,1024]{1,0:T(8,128)(2,1)}, f32[64,128]{1,0:T(8,...) custom-call(bf16[128,1024]{1,0:T(8,128)(2,1)} %refs_0_.3, bf16[64,128]{1,0:T(8,128)(2,1)} %bitcast.74, ...), custom_call_target="tpu_custom_call" | custom-call | flops 4294967296 | bytes 2097152 | tf_op jit(solution)/shard_map/pallas_call | solution.py:567
  227.2 3.7 %shard_map.240 = (bf16[128,1024]{1,0:T(8,128)(2,1)}, f32[64,128]{1,0:T(8,128)}, f32[16,128]{1,0:T(8,128)}) custom-call(bf16[64,8,128]{2,1,0:T(8,128)(2,1)S(1)} %all-to-all-done.7.refs_0_, bf16[64,1024]{1,0:T(8,128)(2,1)} %get-tuple-element.88.refs_6_.refs_1_, bf16[64,128]{1,0:T(8,128)(2,1)} %bitcast.75, f32[16,128]{1,0:T(8,128)} %bitcast.79, ...), custom_call_target="tpu_custom_call" | custom-call | flops 1073741824 | bytes 2097152 | tf_op jit(solution)/shard_map/pallas_call | solution.py:567
  (82 shorter events, 47.2 us)
Async XLA Ops:
  2.8 30.9 %all-to-all-start = ((bf16[64,32,128]{2,1,0:T(8,128)(2,1)}), bf16[64,32,128]{2,1,0:T(8,128)(2,1)S(1)}, u32[]{:S(2)}, u32[]{:S(2)}) async-start(bf16[64,32,128]{2,1,0:T(8,128)(2,1)} %shard_map.223), calls=%async_computation | async-start | bytes 1048576 | tf_op jit(solution)/shard_map/all_to_all | solution.py:30
  33.7 28.7 %all-to-all-start.1 = ((bf16[64,48,128]{2,1,0:T(8,128)(2,1)}), bf16[64,48,128]{2,1,0:T(8,128)(2,1)S(1)}, u32[]{:S(2)}, u32[]{:S(2)}) async-start(bf16[64,48,128]{2,1,0:T(8,128)(2,1)} %shard_map.224), calls=%async_computation.1 | async-start | bytes 1572864 | tf_op jit(solution)/shard_map/all_to_all | solution.py:30
  39.4 25.8 %collective-permute-start = (bf16[512,512]{1,0:T(8,128)(2,1)S(1)}, bf16[512,512]{1,0:T(8,128)(2,1)S(1)}, u32[]{:S(2)}, u32[]{:S(2)}) collective-permute-start(bf16[512,512]{1,0:T(8,128)(2,1)S(1)} %bitcast.53), channel_id=1, source_target_pairs={{0,1},{1,2},{2,3},{3,0},{4,5},{5,6},{6,7},{7,4},{8,9},{9,10},{10,1... | collective-permute-start | bytes 1572872 | tf_op jit(solution)/shard_map/ppermute | solution.py:22
  40.6 33.6 %collective-permute-start.1 = (bf16[512,512]{1,0:T(8,128)(2,1)S(1)}, bf16[512,512]{1,0:T(8,128)(2,1)S(1)}, u32[]{:S(2)}, u32[]{:S(2)}) collective-permute-start(bf16[512,512]{1,0:T(8,128)(2,1)S(1)} %bitcast.54), channel_id=1, source_target_pairs={{0,3},{1,0},{2,1},{3,2},{4,7},{5,4},{6,5},{7,6},{8,11},{9,8},{10,9... | collective-permute-start | bytes 1572872 | tf_op jit(solution)/shard_map/ppermute | solution.py:22
  42.1 32.2 %collective-permute-start.2 = (bf16[512,512]{1,0:T(8,128)(2,1)S(1)}, bf16[512,512]{1,0:T(8,128)(2,1)S(1)}, u32[]{:S(2)}, u32[]{:S(2)}) collective-permute-start(bf16[512,512]{1,0:T(8,128)(2,1)S(1)} %bitcast.55), channel_id=1, source_target_pairs={{0,2},{1,3},{2,0},{3,1},{4,6},{5,7},{6,4},{7,5},{8,10},{9,11},{10,... | collective-permute-start | bytes 1572872 | tf_op jit(solution)/shard_map/ppermute | solution.py:22
  62.4 32.0 %collective-permute-start.3 = (bf16[512,512]{1,0:T(8,128)(2,1)S(1)}, bf16[512,512]{1,0:T(8,128)(2,1)}, u32[]{:S(2)}, u32[]{:S(2)}) collective-permute-start(bf16[512,512]{1,0:T(8,128)(2,1)S(1)} %slice_bitcast_fusion.own_ref.refs_5_), channel_id=1, source_target_pairs={{0,1},{1,2},{2,3},{3,0},{4,5},{5,6},{6,7},{7,4},{8,9},{9,10},{10,1... | collective-permute-start | bytes 1572872 | tf_op jit(solution)/shard_map/ppermute | solution.py:22
  63.7 30.7 %collective-permute-start.4 = (bf16[512,512]{1,0:T(8,128)(2,1)S(1)}, bf16[512,512]{1,0:T(8,128)(2,1)}, u32[]{:S(2)}, u32[]{:S(2)}) collective-permute-start(bf16[512,512]{1,0:T(8,128)(2,1)S(1)} %slice_bitcast_fusion.own_ref.refs_5_), channel_id=1, source_target_pairs={{0,3},{1,0},{2,1},{3,2},{4,7},{5,4},{6,5},{7,6},{8,11},{9,8},{10,9... | collective-permute-start | bytes 1572872 | tf_op jit(solution)/shard_map/ppermute | solution.py:22
  65.2 29.3 %collective-permute-start.5 = (bf16[512,512]{1,0:T(8,128)(2,1)S(1)}, bf16[512,512]{1,0:T(8,128)(2,1)}, u32[]{:S(2)}, u32[]{:S(2)}) collective-permute-start(bf16[512,512]{1,0:T(8,128)(2,1)S(1)} %slice_bitcast_fusion.own_ref.refs_5_), channel_id=1, source_target_pairs={{0,2},{1,3},{2,0},{3,1},{4,6},{5,7},{6,4},{7,5},{8,10},{9,11},{10,... | collective-permute-start | bytes 1572872 | tf_op jit(solution)/shard_map/ppermute | solution.py:22
  67.5 17.8 %all-to-all-start.2 = ((bf16[64,8,128]{2,1,0:T(8,128)(2,1)}), bf16[64,8,128]{2,1,0:T(8,128)(2,1)S(1)}, u32[]{:S(2)}, u32[]{:S(2)}) async-start(bf16[64,8,128]{2,1,0:T(8,128)(2,1)} %copy-done.9), calls=%async_computation.2 | async-start | bytes 262144 | tf_op jit(solution)/shard_map/all_to_all | solution.py:30
  90.0 37.0 %all-to-all-start.3 = ((bf16[4,128,1024]{2,1,0:T(8,128)(2,1)}), bf16[4,128,1024]{2,1,0:T(8,128)(2,1)}, u32[]{:S(2)}, u32[]{:S(2)}) async-start(bf16[4,128,1024]{2,1,0:T(8,128)(2,1)} %broadcast_in_dim.34), calls=%async_computation.3 | async-start | bytes 2097152 | tf_op jit(solution)/shard_map/all_to_all | solution.py:30
  101.8 14.9 %collective-permute-start.6 = (bf16[512,512]{1,0:T(8,128)(2,1)S(1)}, bf16[512,512]{1,0:T(8,128)(2,1)S(1)}, u32[]{:S(2)}, u32[]{:S(2)}) collective-permute-start(bf16[512,512]{1,0:T(8,128)(2,1)S(1)} %get-tuple-element.69), channel_id=1, source_target_pairs={{0,1},{1,2},{2,3},{3,0},{4,5},{5,6},{6,7},{7,4},{8,9},{9,10},{10,1... | collective-permute-start | bytes 1572872 | tf_op jit(solution)/shard_map/ppermute | solution.py:22
  102.1 14.6 %collective-permute-start.7 = (bf16[512,512]{1,0:T(8,128)(2,1)S(1)}, bf16[512,512]{1,0:T(8,128)(2,1)S(1)}, u32[]{:S(2)}, u32[]{:S(2)}) collective-permute-start(bf16[512,512]{1,0:T(8,128)(2,1)S(1)} %get-tuple-element.70), channel_id=1, source_target_pairs={{0,3},{1,0},{2,1},{3,2},{4,7},{5,4},{6,5},{7,6},{8,11},{9,8},{10,9... | collective-permute-start | bytes 1572872 | tf_op jit(solution)/shard_map/ppermute | solution.py:22
  104.5 22.3 %collective-permute-start.8 = (bf16[512,512]{1,0:T(8,128)(2,1)S(1)}, bf16[512,512]{1,0:T(8,128)(2,1)S(1)}, u32[]{:S(2)}, u32[]{:S(2)}) collective-permute-start(bf16[512,512]{1,0:T(8,128)(2,1)S(1)} %get-tuple-element.71), channel_id=1, source_target_pairs={{0,2},{1,3},{2,0},{3,1},{4,6},{5,7},{6,4},{7,5},{8,10},{9,11},{10,... | collective-permute-start | bytes 1572872 | tf_op jit(solution)/shard_map/ppermute | solution.py:22
  155.8 12.8 %all-to-all-start.5 = ((bf16[4,128,512]{2,1,0:T(8,128)(2,1)}), bf16[4,128,512]{2,1,0:T(8,128)(2,1)S(1)}, u32[]{:S(2)}, u32[]{:S(2)}) async-start(bf16[4,128,512]{2,1,0:T(8,128)(2,1)} %shard_map.234), calls=%async_computation.5 | async-start | bytes 1048576 | tf_op jit(solution)/shard_map/all_to_all | solution.py:30
  159.7 32.4 %collective-permute-start.13 = (bf16[4,128,1024]{2,1,0:T(8,128)(2,1)}, bf16[4,128,1024]{2,1,0:T(8,128)(2,1)S(1)}, u32[]{:S(2)}, u32[]{:S(2)}) collective-permute-start(bf16[4,128,1024]{2,1,0:T(8,128)(2,1)} %all-to-all-done.3.refs_5_), channel_id=1, source_target_pairs={{0,4},{4,0},{1,5},{5,1},{2,6},{6,2},{3,7},{7,3},{8,12},{12,8},{9,1... | collective-permute-start | bytes 3145736 | tf_op jit(solution)/shard_map/ppermute | solution.py:22
  169.0 12.2 %collective-permute-start.9 = (bf16[4,8,32,128]{3,2,0,1:T(8,128)(2,1)S(1)}, bf16[4,8,32,128]{3,2,0,1:T(8,128)(2,1)S(1)}, u32[]{:S(2)}, u32[]{:S(2)}) collective-permute-start(bf16[4,8,32,128]{3,2,0,1:T(8,128)(2,1)S(1)} %get-tuple-element.105), channel_id=1, source_target_pairs={{0,4},{4,0},{1,5},{5,1},{2,6},{6,2},{3,7},{7,3},{8,12},{12,8},{9,1... | collective-permute-start | bytes 786440 | tf_op jit(solution)/shard_map/ppermute | solution.py:22
  176.1 24.5 %all-to-all-start.6 = ((bf16[64,8,128]{2,1,0:T(8,128)(2,1)}), bf16[64,8,128]{2,1,0:T(8,128)(2,1)S(1)}, u32[]{:S(2)}, u32[]{:S(2)}) async-start(bf16[64,8,128]{2,1,0:T(8,128)(2,1)} %get-tuple-element.87), calls=%async_computation.6 | async-start | bytes 262144 | tf_op jit(solution)/shard_map/all_to_all | solution.py:30
  181.3 10.8 %collective-permute-start.10 = (bf16[2,8,32,128]{3,2,1,0:T(8,128)(2,1)S(1)}, bf16[2,8,32,128]{3,2,1,0:T(8,128)(2,1)S(1)}, u32[]{:S(2)}, u32[]{:S(2)}) collective-permute-start(bf16[2,8,32,128]{3,2,1,0:T(8,128)(2,1)S(1)} %get-tuple-element.103), channel_id=1, source_target_pairs={{0,8},{8,16},{16,24},{24,0},{1,9},{9,17},{17,25},{25,1},{2,10},{10... | collective-permute-start | bytes 393224 | tf_op jit(solution)/shard_map/ppermute | solution.py:22
  194.9 23.5 %collective-permute-start.14 = (bf16[32,1024]{1,0:T(8,128)(2,1)S(1)}, bf16[32,1024]{1,0:T(8,128)(2,1)S(1)}, u32[]{:S(2)}, u32[]{:S(2)}) collective-permute-start(bf16[32,1024]{1,0:T(8,128)(2,1)S(1)} %get-tuple-element.76), channel_id=1, source_target_pairs={{0,128},{32,160},{64,192},{96,224},{128,0},{160,32},{192,64},{224,... | collective-permute-start | bytes 196616 | tf_op jit(solution)/shard_map/ppermute | solution.py:22
  200.0 18.8 %collective-permute-start.15 = (bf16[32,1024]{1,0:T(8,128)(2,1)S(1)}, bf16[32,1024]{1,0:T(8,128)(2,1)S(1)}, u32[]{:S(2)}, u32[]{:S(2)}) collective-permute-start(bf16[32,1024]{1,0:T(8,128)(2,1)S(1)} %get-tuple-element.77), channel_id=1, source_target_pairs={{0,96},{32,128},{64,160},{96,192},{128,224},{160,0},{192,32},{224,... | collective-permute-start | bytes 196616 | tf_op jit(solution)/shard_map/ppermute | solution.py:22
  201.4 25.8 %all-to-all-start.7 = ((bf16[64,8,128]{2,1,0:T(8,128)(2,1)}), bf16[64,8,128]{2,1,0:T(8,128)(2,1)S(1)}, u32[]{:S(2)}, u32[]{:S(2)}) async-start(bf16[64,8,128]{2,1,0:T(8,128)(2,1)} %shard_map.238), calls=%async_computation.7 | async-start | bytes 262144 | tf_op jit(solution)/shard_map/all_to_all | solution.py:30
  210.2 16.2 %collective-permute-start.16 = (bf16[32,1024]{1,0:T(8,128)(2,1)S(1)}, bf16[32,1024]{1,0:T(8,128)(2,1)S(1)}, u32[]{:S(2)}, u32[]{:S(2)}) collective-permute-start(bf16[32,1024]{1,0:T(8,128)(2,1)S(1)} %get-tuple-element.78), channel_id=1, source_target_pairs={{0,160},{32,192},{64,224},{96,0},{128,32},{160,64},{192,96},{224,1... | collective-permute-start | bytes 196616 | tf_op jit(solution)/shard_map/ppermute | solution.py:22
  214.8 11.6 %collective-permute-start.17 = (bf16[32,1024]{1,0:T(8,128)(2,1)S(1)}, bf16[32,1024]{1,0:T(8,128)(2,1)S(1)}, u32[]{:S(2)}, u32[]{:S(2)}) collective-permute-start(bf16[32,1024]{1,0:T(8,128)(2,1)S(1)} %get-tuple-element.79), channel_id=1, source_target_pairs={{0,64},{32,96},{64,128},{96,160},{128,192},{160,224},{192,0},{224,... | collective-permute-start | bytes 196616 | tf_op jit(solution)/shard_map/ppermute | solution.py:22
  215.2 11.2 %collective-permute-start.18 = (bf16[32,1024]{1,0:T(8,128)(2,1)S(1)}, bf16[32,1024]{1,0:T(8,128)(2,1)S(1)}, u32[]{:S(2)}, u32[]{:S(2)}) collective-permute-start(bf16[32,1024]{1,0:T(8,128)(2,1)S(1)} %get-tuple-element.80), channel_id=1, source_target_pairs={{0,192},{32,224},{64,0},{96,32},{128,64},{160,96},{192,128},{224,1... | collective-permute-start | bytes 196616 | tf_op jit(solution)/shard_map/ppermute | solution.py:22
  (16 other events, 189.8 us)
